TPU v7x, 32 devices: a whole 2x2x4 slice. The times are simulated.
32 devices in a mesh: ep: 8 (over z, core), tp: 4 (over y, x).
Axes of the slice: x: 2, y: 2, z: 4, core: 2. Of those that a mesh axis runs over, the one named last changes fastest.
Arguments:
- queries: bfloat16 [2048, 2048], P('ep', 'tp'), may hold values from -6 to 6
- keys: bfloat16 [2048, 2048], P('ep', 'tp'), may hold values from -6 to 6
- values: bfloat16 [2048, 2048], P('ep', 'tp'), may hold values from -6 to 6
- gates: bfloat16 [2048, 2048], P('ep', 'tp'), may hold values from -6 to 6
- log_decay: float32 [2048, 16], P('ep', 'tp'), may hold values from -2 to 0
- out_weight: bfloat16 [2048, 2048], P(None, 'tp'), may hold values from -0.125 to 0.125
- moe_rows: bfloat16 [2048, 2048], P('ep'), may hold values from -140 to 140
- moe_gain: bfloat16 [2048], replicated, may hold values from 0.099609375 to 1.8984375
- routes: int32 [2048, 2], P('ep'), may hold values from 0 to 7, as said below
- route_weights: float32 [2048, 2], P('ep'), may hold values from 0.1 to 1
- gate_proj: bfloat16 [8, 2048, 4096], P('ep', None, 'tp'), may hold values from -0.125 to 0.125
- up_proj: bfloat16 [8, 2048, 4096], P('ep', None, 'tp'), may hold values from -0.125 to 0.125
- down_proj: bfloat16 [8, 4096, 2048], P('ep', None, 'tp'), may hold values from -0.09375 to 0.09375
Outputs:
- mixer_out: bfloat16 [2048, 2048], P('ep', 'tp')
- moe_out: bfloat16 [2048, 2048], P('ep', 'tp')
Inputs may be any that keep to these rules, and one draw needn't show every extreme that they name: `routes`: each row names two different experts of one group of 8 consecutive experts; in each aligned block of 256 rows every expert is named by exactly 64 rows.
All inputs are finite; a program needn't handle non-finite values.
Results may differ from a plain program's by a relative error of at most 0.011.
Values may be sent and summed in bfloat16 or wider, within the bound.
A program may use at most 64 MiB of HBM per device.

v0:
```python
import functools

import jax
import jax.numpy as jnp
from jax import lax
from jax.experimental import pallas as pl
from jax.experimental.pallas import tpu as pltpu
from jax.sharding import PartitionSpec as P

BLOCK = 128
CHUNKS = 2
MESH = pl.DeviceIdType.MESH
F32 = jnp.float32
BF16 = jnp.bfloat16


def each(low, high, body):
    if high - low <= 8:
        for index in range(low, high):
            body(index)
    else:

        @pl.loop(low, high)
        def _(index):
            body(index)


def span(index, size):
    return pl.ds(pl.multiple_of(index * size, size), size)


def split(value):
    high = value.astype(BF16)
    return high, (value - high.astype(F32)).astype(BF16)


def dot(a, b, dims=((1,), (0,))):
    return lax.dot_general(a, b, (dims, ((), ())), preferred_element_type=F32)


class Gather:
    def __init__(self, tp, region, half, send, recv):
        self.tp, self.region, self.half, self.send, self.recv = tp, region, half, send, recv
        self.me = lax.axis_index("tp")

    def copy(self, ref, slot, to):
        return pltpu.make_async_remote_copy(
            src_ref=ref, dst_ref=ref, send_sem=self.send(slot), recv_sem=self.recv(slot),
            device_id={"tp": to}, device_id_type=MESH,
        )

    def outs(self):
        me, tp = self.me, self.tp
        if tp == 4:
            return [self.copy(self.region(me), k - 1, me ^ k) for k in (1, 2)]
        return [self.copy(self.region(me), k - 1, lax.rem(me + k, tp)) for k in range(1, tp)]

    def hops(self):
        me = self.me
        return [
            self.copy(self.half(me ^ 1, 0), 2, me ^ 2),
            self.copy(self.half(me ^ 2, 1), 3, me ^ 1),
        ]

    def start(self):
        for copy in self.outs():
            copy.start()

    def forward(self):
        if self.tp == 4:
            me = self.me
            hops = self.hops()
            for k in (1, 2):
                self.copy(self.region(me ^ k), k - 1, me ^ k).wait_recv()
                hops[k - 1].start()

    def finish(self):
        me, tp = self.me, self.tp
        if tp == 4:
            self.copy(self.half(me ^ 3, 0), 2, me ^ 2).wait_recv()
            self.copy(self.half(me ^ 3, 1), 3, me ^ 1).wait_recv()
        else:
            for k in range(1, tp):
                owner = lax.rem(me + tp - k, tp)
                self.copy(self.region(owner), k - 1, owner).wait_recv()

    def drain(self):
        for copy in self.outs() + (self.hops() if self.tp == 4 else []):
            copy.wait_send()


def kernel(
    ep, tp,
    q_ref, k_ref, v_ref, g_ref, ld_ref, cos_ref, sin_ref, rows_ref, gain_ref, routes_ref, rw_ref,
    wo_hbm, wg_hbm, wu_hbm, wd_hbm,
    mix_ref, moe_ref,
    wo, wg, wu, wd, normed, p0, p1, og, partner_rows, x, h, eo, ret, ho, state, landed, excl,
    rq, inside, cums, pack, narrow,
    w_sem, z_send, z_recv, f_send, f_recv, h_send, h_recv, r_send, r_recv, m_send, m_recv,
    s_send, s_recv,
):
    e, t = lax.axis_index("ep"), lax.axis_index("tp")
    rows, d = rows_ref.shape
    cap = 2 * rows // ep
    dq = d // tp
    ff = wd.shape[0]
    fq = ff // tp
    heads = ld_ref.shape[0]
    hd = q_ref.shape[1] // heads
    blocks = rows // BLOCK
    chunk = ep * cap // CHUNKS
    half_ep = ep // CHUNKS
    pieces = 2 if fq >= 512 else 1
    piece = fq // pieces

    barrier = pltpu.get_barrier_semaphore()

    def greet_ep(off):
        pl.semaphore_signal(barrier, inc=1, device_id={"ep": e ^ off}, device_id_type=MESH)

    each(1, ep, greet_ep)
    for k in range(1, tp):
        pl.semaphore_signal(
            barrier, inc=1, device_id={"tp": lax.rem(t + k, tp)}, device_id_type=MESH
        )

    loads = [
        pltpu.make_async_copy(src, dst, w_sem.at[i])
        for i, (src, dst) in enumerate(
            ((wg_hbm.at[0], wg), (wu_hbm.at[0], wu), (wd_hbm.at[0], wd), (wo_hbm, wo))
        )
    ]
    for load in loads:
        load.start()

    pack[...] = jnp.zeros_like(pack)
    pack[0:2, :] = routes_ref[...].astype(F32)
    pack[2:4, :] = rw_ref[...]
    pack[4 : 4 + heads, :] = ld_ref[...]
    for b in range(rows // 128):
        narrow[b * 128 : (b + 1) * 128, :] = pack[:, b * 128 : (b + 1) * 128].T
    routes = [narrow[:, k : k + 1].astype(jnp.int32) for k in range(2)]

    step_rows = 32

    @pl.loop(0, rows // step_rows)
    def _(i):
        at = span(i, step_rows)
        val = rows_ref[at, :].astype(F32)
        scale = lax.rsqrt(jnp.mean(val * val, axis=-1, keepdims=True) + 1e-06)
        for c in range(d // 128):
            cols = slice(c * 128, (c + 1) * 128)
            normed[at, cols] = (val[:, cols] * scale * gain_ref[c : c + 1, :].astype(F32)).astype(
                BF16
            )

    lanes = lax.broadcasted_iota(jnp.int32, (rows, 128), 1)
    hot = [(routes[k] == lanes).astype(F32) for k in range(2)]
    before = (
        lax.broadcasted_iota(jnp.int32, (rows, rows), 0)
        > lax.broadcasted_iota(jnp.int32, (rows, rows), 1)
    ).astype(F32).astype(BF16)
    rank = dot(before, (hot[0] + hot[1]).astype(BF16))
    slots = lax.broadcasted_iota(jnp.int32, (rows, ep * cap), 1)
    small = lax.broadcasted_iota(jnp.int32, (rows, cap), 1)
    targets = []
    for k, ref in ((0, p0), (1, p1)):
        target = routes[k] * cap + jnp.sum(
            rank * hot[k], axis=1, keepdims=True
        ).astype(jnp.int32)
        targets.append(target)
        ref[...] = (slots == target).astype(F32).astype(BF16)
    both = p0[...] + p1[...]
    og[...] = dot(both, normed[:, span(t, dq)], ((0,), (0,))).astype(BF16)

    def block_of(dest):
        base = small + dest * cap
        return ((base == targets[0]) | (base == targets[1])).astype(F32).astype(BF16)

    partner_rows[...] = dot(block_of(e ^ 1), normed[...], ((0,), (0,))).astype(BF16)
    x[span(e, cap), :] = dot(block_of(e), normed[...], ((0,), (0,))).astype(BF16)

    pl.semaphore_wait(barrier, ep - 1 + tp - 1)

    def z_copy(off, here):
        other = e ^ off
        if isinstance(off, int) and off == 1:
            src, dst = partner_rows, x.at[span(other if here else e, cap), :]
        else:
            src = og.at[span(other, cap), :]
            dst = x.at[span(other if here else e, cap), span(t, dq)]
        return pltpu.make_async_remote_copy(
            src_ref=src, dst_ref=dst, send_sem=z_send.at[other],
            recv_sem=z_recv.at[other if here else e],
            device_id={"ep": other}, device_id_type=MESH,
        )

    z_copy(1, False).start()
    each(2, ep, lambda off: z_copy(off, False).start())

    row_i = lax.broadcasted_iota(jnp.int32, (BLOCK, BLOCK), 0)
    col_j = lax.broadcasted_iota(jnp.int32, (BLOCK, BLOCK), 1)
    causal = row_i >= col_j
    lower = causal.astype(F32)
    factor = hd ** (-0.5)
    for b in range(blocks):
        at = slice(b * BLOCK, (b + 1) * BLOCK)
        cums[at, :] = lax.dot_general(
            lower, narrow[at, :], (((1,), (0,)), ((), ())),
            preferred_element_type=F32, precision=lax.Precision.HIGHEST,
        )
    decay_at = heads * hd
    for n in range(heads):
        cols = slice(n * hd, (n + 1) * hd)
        total = None
        gone = None
        for b in range(blocks):
            at = slice(b * BLOCK, (b + 1) * BLOCK)
            cos, sin = cos_ref[at, :], sin_ref[at, :]

            def turned(ref):
                val = ref[at, cols].astype(F32)
                return val * cos + pltpu.roll(val, hd // 2, 1) * sin

            qb = turned(q_ref).astype(BF16)
            kb = (turned(k_ref) * factor).astype(BF16)
            vb = v_ref[at, cols]
            rq[at, cols] = qb
            cum = jnp.broadcast_to(cums[at, 4 + n : 5 + n], (BLOCK, BLOCK))
            spread = cum - cum.T
            weight = jnp.where(causal, jnp.exp(jnp.where(causal, spread, 0.0)), 0.0)
            scores = dot(qb, kb, ((1,), (1,)))
            inside[at, cols] = dot((scores * weight).astype(BF16), vb)
            ending = cum[BLOCK - 1 : BLOCK, :]
            k_hi, k_lo = split(kb.astype(F32) * jnp.exp(ending - cum))
            update = dot(k_hi, vb, ((0,), (0,))) + dot(k_lo, vb, ((0,), (0,)))
            if b == 0:
                total, gone = update, ending
            else:
                if b < blocks:
                    pass
                total = jnp.exp(ending) * total + update
                gone = gone + ending
            if b < blocks - 1:
                excl[1 + b, n * hd : (n + 1) * hd, :] = total
        state[0, n * hd : (n + 1) * hd, :] = total
        state[0, decay_at + n : decay_at + n + 1, :] = jnp.exp(gone)

    excl[0, :decay_at, :] = jnp.zeros((decay_at, hd), F32)
    excl[0, decay_at : decay_at + heads, :] = jnp.ones((heads, hd), F32)

    rounds = state.shape[0]

    def s_copy(r):
        return pltpu.make_async_remote_copy(
            src_ref=state.at[r], dst_ref=landed.at[r], send_sem=s_send.at[r],
            recv_sem=s_recv.at[r], device_id={"ep": lax.rem(e + 2**r, ep)}, device_id_type=MESH,
        )

    def scan_send(r):
        @pl.when(e + 2**r < ep)
        def _():
            s_copy(r).start()

    def scan_take(r):
        last = r == rounds - 1

        @pl.when(e >= 2**r)
        def _():
            s_copy(r).wait_recv()
            for n in range(heads):
                at = slice(n * hd, (n + 1) * hd)
                da = slice(decay_at + n, decay_at + n + 1)
                came, came_d = landed[r, at, :], landed[r, da, :]
                own_d = excl[0, da, :]
                excl[0, at, :] = own_d * came + excl[0, at, :]
                excl[0, da, :] = own_d * came_d
                if not last:
                    mine_d = state[r, da, :]
                    state[r + 1, at, :] = mine_d * came + state[r, at, :]
                    state[r + 1, da, :] = mine_d * came_d

        if not last:

            @pl.when(e < 2**r)
            def _():
                state[r + 1, : decay_at + heads, :] = state[r, : decay_at + heads, :]

    def row_gather(off):
        other = e ^ off
        start = other * cap

        def half(owner, k):
            return x.at[
                pl.ds(pl.multiple_of(start + k * (cap // 2), cap // 2), cap // 2), span(owner, dq)
            ]

        return Gather(
            tp, lambda owner: x.at[span(other, cap), span(owner, dq)], half,
            lambda slot: f_send.at[other, slot], lambda slot: f_recv.at[other, slot],
        )

    def part_of(c):
        return (e // half_ep) ^ c

    def hid_gather(c, j):
        base = part_of(c) * chunk

        def cols(owner):
            return pl.ds(pl.multiple_of(owner * fq + j * piece, piece), piece)

        return Gather(
            tp,
            lambda owner: h.at[pl.ds(pl.multiple_of(base, chunk), chunk), cols(owner)],
            lambda owner, k: h.at[
                pl.ds(pl.multiple_of(base + k * (chunk // 2), chunk // 2), chunk // 2), cols(owner)
            ],
            lambda slot: h_send.at[c * pieces + j, slot],
            lambda slot: h_recv.at[c * pieces + j, slot],
        )

    mix_gather = Gather(
        tp, lambda owner: ho.at[:, span(owner, heads * hd)],
        lambda owner, k: ho.at[k * (rows // 2) : (k + 1) * (rows // 2), span(owner, heads * hd)],
        lambda slot: m_send.at[slot], lambda slot: m_recv.at[slot],
    )

    def take_rows(off):
        z_copy(off, True).wait_recv()
        row_gather(off).start()

    def hidden_piece(c, j):
        at = pl.ds(pl.multiple_of(part_of(c) * chunk, chunk), chunk)
        tile = min(256, piece)

        @pl.loop(0, piece // tile)
        def _(i):
            cols = pl.ds(pl.multiple_of(j * piece + i * tile, tile), tile)
            held = x[at, :]
            gate = dot(held, wg[:, cols])
            up = dot(held, wu[:, cols])
            hid = (gate / (1.0 + jnp.exp(-gate)) * up).astype(BF16)
            h[at, pl.ds(pl.multiple_of(t * fq + j * piece + i * tile, tile), tile)] = hid

        hid_gather(c, j).start()

    def back_copy(off, here):
        other = e ^ off
        return pltpu.make_async_remote_copy(
            src_ref=eo.at[span(other, cap), :], dst_ref=ret.at[span(other if here else e, cap), :],
            send_sem=r_send.at[other], recv_sem=r_recv.at[other if here else e],
            device_id={"ep": other}, device_id_type=MESH,
        )

    def down(c):
        at = pl.ds(pl.multiple_of(part_of(c) * chunk, chunk), chunk)
        tile = min(256, dq)

        @pl.loop(0, dq // tile)
        def _(i):
            cols = pl.ds(pl.multiple_of(i * tile, tile), tile)
            eo[at, cols] = dot(h[at, :], wd[:, cols]).astype(BF16)

        if c == 0:
            ret[span(e, cap), :] = eo[span(e, cap), :]
        each(max(1, c * half_ep), (c + 1) * half_ep, lambda off: back_copy(off, False).start())

    scan_send(0)
    each(2, half_ep, take_rows)
    each(half_ep, ep, take_rows)
    scan_take(0)
    if rounds > 1:
        scan_send(1)
    each(2, half_ep, lambda off: row_gather(off).forward())
    loads[0].wait()
    loads[1].wait()
    z_copy(1, True).wait_recv()
    each(2, half_ep, lambda off: row_gather(off).finish())
    hidden_piece(0, 0)
    each(half_ep, ep, lambda off: row_gather(off).forward())
    for j in range(1, pieces):
        hidden_piece(0, j)
    if rounds > 1:
        scan_take(1)
    if rounds > 2:
        scan_send(2)
    each(half_ep, ep, lambda off: row_gather(off).finish())
    hid_gather(0, 0).forward()
    hidden_piece(1, 0)
    for j in range(1, pieces):
        hid_gather(0, j).forward()
    for j in range(1, pieces):
        hidden_piece(1, j)
    for r in range(2, rounds):
        scan_take(r)
        if r + 1 < rounds:
            scan_send(r + 1)

    for n in range(heads):
        cols = slice(n * hd, (n + 1) * hd)
        sat = slice(n * hd, (n + 1) * hd)
        entering = excl[0, sat, :]
        gone = None
        for b in range(blocks):
            at = slice(b * BLOCK, (b + 1) * BLOCK)
            cum = jnp.broadcast_to(cums[at, 4 + n : 5 + n], (BLOCK, hd))
            held = entering if b == 0 else jnp.exp(gone) * entering + excl[b, sat, :]
            hi, lo = split(held)
            qb = rq[at, cols]
            retained = inside[at, cols] + (dot(qb, hi) + dot(qb, lo)) * jnp.exp(cum)
            scale = lax.rsqrt(jnp.mean(retained * retained, axis=-1, keepdims=True) + 1e-05)
            gate = g_ref[at, cols].astype(F32)
            out = (retained * scale * (gate / (1.0 + jnp.exp(-gate)))).astype(BF16)
            ho[at, pl.ds(pl.multiple_of(t * heads * hd + n * hd, hd), hd)] = out
            ending = cum[BLOCK - 1 : BLOCK, :]
            gone = ending if gone is None else gone + ending
    mix_gather.start()

    loads[2].wait()
    loads[3].wait()
    for j in range(pieces):
        hid_gather(0, j).finish()
    hid_gather(1, 0).forward()
    down(0)
    for j in range(1, pieces):
        hid_gather(1, j).forward()
    mix_gather.forward()
    for j in range(pieces):
        hid_gather(1, j).finish()
    down(1)
    mix_gather.finish()
    tile = min(256, dq)

    @pl.loop(0, dq // tile)
    def _(i):
        cols = pl.ds(pl.multiple_of(i * tile, tile), tile)
        mix_ref[:, cols] = dot(ho[...], wo[:, cols]).astype(BF16)

    each(1, ep, lambda off: back_copy(off, True).wait_recv())

    @pl.loop(0, dq // tile)
    def _(i):
        cols = pl.ds(pl.multiple_of(i * tile, tile), tile)
        came = ret[:, cols]
        moe_ref[:, cols] = (
            dot(p0[...], came) * narrow[:, 2:3] + dot(p1[...], came) * narrow[:, 3:4]
        ).astype(BF16)

    z_copy(1, False).wait_send()
    each(2, ep, lambda off: z_copy(off, False).wait_send())
    each(2, ep, lambda off: row_gather(off).drain())
    each(1, ep, lambda off: back_copy(off, False).wait_send())
    for c in range(CHUNKS):
        for j in range(pieces):
            hid_gather(c, j).drain()
    mix_gather.drain()
    for r in range(rounds):

        @pl.when(e + 2**r < ep)
        def _():
            s_copy(r).wait_send()


def on_device(
    ep, tp,
    queries, keys, values, gates, log_decay, out_weight, moe_rows, moe_gain, routes,
    route_weights, gate_proj, up_proj, down_proj,
):
    rows, d = moe_rows.shape
    heads = log_decay.shape[1]
    width = queries.shape[1]
    hd = width // heads
    cap = 2 * rows // ep
    dq = d // tp
    fq = gate_proj.shape[2]
    ff = down_proj.shape[1]
    rounds = (ep - 1).bit_length()
    slots = max(4, tp - 1)
    pieces = CHUNKS * 2
    blocks = rows // BLOCK
    positions = (lax.axis_index("ep") * rows + jnp.arange(rows, dtype=jnp.int32)).astype(F32)
    half = hd // 2
    inverse = 10000.0 ** (-jnp.arange(half, dtype=F32) / half)
    angles = positions[:, None] * jnp.tile(inverse, 2)[None, :]
    sign = jnp.where(jnp.arange(hd) < half, -1.0, 1.0).astype(F32)
    cos, sin = jnp.cos(angles), jnp.sin(angles) * sign[None, :]
    srows = heads * hd + 8 * ((heads + 7) // 8)
    vmem = pl.BlockSpec(memory_space=pltpu.VMEM)
    hbm = pl.BlockSpec(memory_space=pl.ANY)
    dma = pltpu.SemaphoreType.DMA
    out = jax.ShapeDtypeStruct((rows, dq), BF16)
    return pl.pallas_call(
        functools.partial(kernel, ep, tp),
        out_shape=(out, out),
        in_specs=[vmem] * 11 + [hbm] * 4,
        out_specs=(vmem, vmem),
        scratch_shapes=[
            pltpu.VMEM(out_weight.shape, BF16),
            pltpu.VMEM((d, fq), BF16),
            pltpu.VMEM((d, fq), BF16),
            pltpu.VMEM((ff, dq), BF16),
            pltpu.VMEM((rows, d), BF16),
            pltpu.VMEM((rows, ep * cap), BF16),
            pltpu.VMEM((rows, ep * cap), BF16),
            pltpu.VMEM((ep * cap, dq), BF16),
            pltpu.VMEM((cap, d), BF16),
            pltpu.VMEM((ep * cap, d), BF16),
            pltpu.VMEM((ep * cap, ff), BF16),
            pltpu.VMEM((ep * cap, dq), BF16),
            pltpu.VMEM((ep * cap, dq), BF16),
            pltpu.VMEM((rows, width * tp), BF16),
            pltpu.VMEM((rounds, srows, hd), F32),
            pltpu.VMEM((rounds, srows, hd), F32),
            pltpu.VMEM((blocks, srows, hd), F32),
            pltpu.VMEM((rows, width), BF16),
            pltpu.VMEM((rows, width), F32),
            pltpu.VMEM((rows, 128), F32),
            pltpu.VMEM((128, rows), F32),
            pltpu.VMEM((rows, 128), F32),
            dma((4,)),
            dma((ep,)), dma((ep,)),
            dma((ep, slots)), dma((ep, slots)),
            dma((pieces, slots)), dma((pieces, slots)),
            dma((ep,)), dma((ep,)),
            dma((slots,)), dma((slots,)),
            dma((rounds,)), dma((rounds,)),
        ],
        compiler_params=pltpu.CompilerParams(
            collective_id=0, has_side_effects=True, vmem_limit_bytes=60 * 1024 * 1024
        ),
    )(
        queries, keys, values, gates, log_decay.T, cos, sin, moe_rows, moe_gain.reshape(-1, 128),
        routes.T, route_weights.T, out_weight, gate_proj, up_proj, down_proj,
    )


def solution(mesh):
    placed = (
        P("ep", "tp"), P("ep", "tp"), P("ep", "tp"), P("ep", "tp"), P("ep", "tp"),
        P(None, "tp"), P("ep", None), P(), P("ep", None), P("ep", None),
        P("ep", None, "tp"), P("ep", None, "tp"), P("ep", None, "tp"),
    )
    return jax.shard_map(
        functools.partial(on_device, mesh.shape["ep"], mesh.shape["tp"]),
        mesh=mesh, in_specs=placed, out_specs=(P("ep", "tp"), P("ep", "tp")), check_vma=False,
    )
```

profile of v0, /device:TPU:0, one launch (start us, length us, event | category | flops | bytes accessed | tf_op | source)
XLA Modules:
  0.0 89.7 jit_solution(14856713039399539993)
XLA Ops:
  0.7 0.1 mul.28
  0.8 1.2 %fusion = (f32[256,128]{1,0:T(8,128)}, f32[256,128]{1,0:T(8,128)}) fusion(f32[128]{0:T(128)S(1)} %compare_select_fusion, f32[128]{0:T(128)S(1)} %mul.28, f32[256]{0:T(256)S(1)} %add_convert_fusion), kind=kLoop, calls=%fused_computation.2 | loop fusion | flops 65536 | bytes 264192 | tf_op jit(solution)/shard_map/mul | solution.py:486
  2.0 84.3 %shard_map.140 = (bf16[256,512]{1,0:T(8,128)(2,1)}, bf16[256,512]{1,0:T(8,128)(2,1)}) custom-call(bf16[256,512]{1,0:T(8,128)(2,1)} %q_ref.1, bf16[256,512]{1,0:T(8,128)(2,1)} %k_ref.1, bf16[256,512]{1,0:T(8,128)(2,1)} %v_ref.1, bf16[256,512]{1,0:T(8,128)(2,1)} %g_ref.1, f32[4,256]{1,0:T(4,128)} %bitcast.4, f32[256,128]{1,0:T(8,128)} %get-tuple-element.3.cos_ref, ...), custom_call_target="tpu_custom_call" | custom-call | tf_op jit(solution)/shard_map/pallas_call | solution.py:492
  86.3 1.7 %copy.17 = bf16[256,512]{1,0:T(8,128)(2,1)} copy(bf16[256,512]{1,0:T(8,128)(2,1)} %get-tuple-element.6) | data formatting | bytes 524288
  88.0 1.7 %copy.18 = bf16[256,512]{1,0:T(8,128)(2,1)} copy(bf16[256,512]{1,0:T(8,128)(2,1)} %get-tuple-element.7) | data formatting | bytes 524288
  (4 shorter events, 0.0 us)
where the time goes:
time: 90.3 us; the launch traced here: 89.7 us
  Pallas kernels  84.3 us (93%)
  local copies, waits for them, and re-layouts  3.42 us (4%)
  other arithmetic  1.26 us (1%)
    pallas_call x1, Pallas kernels, on_device(): pl.pallas_call(functools.partial(kernel, ep, tp), out_shape=(out, out), i...  84.3 us
    unnamed x2, local copies, waits for them, and re-layouts  3.34 us

commit v1 on v0

v1 whole, which is shorter than its diff:
```python
import functools

import jax
import jax.numpy as jnp
import numpy as np
from jax import lax
from jax.experimental import pallas as pl
from jax.experimental.pallas import tpu as pltpu
from jax.sharding import PartitionSpec as P

BLOCK = 128
MESH = pl.DeviceIdType.MESH
F32 = jnp.float32
BF16 = jnp.bfloat16


def each(low, high, body):
    if high - low <= 8:
        for index in range(low, high):
            body(index)
    else:

        @pl.loop(low, high)
        def _(index):
            body(index)


def span(index, size):
    return pl.ds(pl.multiple_of(index * size, size), size)


def split(value):
    high = value.astype(BF16)
    return high, (value - high.astype(F32)).astype(BF16)


def dot(a, b, dims=((1,), (0,))):
    return lax.dot_general(a, b, (dims, ((), ())), preferred_element_type=F32)


def chunk_units(ep):
    g = ep // 4
    return [(0, g), (2 * g, g), (g, g), (3 * g, g // 2), (3 * g + g // 2, g // 2)]


class Gather:
    def __init__(self, tp, region, half, send, recv):
        self.tp, self.region, self.half, self.send, self.recv = tp, region, half, send, recv
        self.me = lax.axis_index("tp")

    def copy(self, ref, slot, to):
        return pltpu.make_async_remote_copy(
            src_ref=ref, dst_ref=ref, send_sem=self.send(slot), recv_sem=self.recv(slot),
            device_id={"tp": to}, device_id_type=MESH,
        )

    def outs(self):
        me, tp = self.me, self.tp
        if tp == 4:
            return [self.copy(self.region(me), k - 1, me ^ k) for k in (1, 2)]
        return [self.copy(self.region(me), k - 1, lax.rem(me + k, tp)) for k in range(1, tp)]

    def hops(self):
        me = self.me
        return [
            self.copy(self.half(me ^ 1, 0), 2, me ^ 2),
            self.copy(self.half(me ^ 2, 1), 3, me ^ 1),
        ]

    def start(self):
        for copy in self.outs():
            copy.start()

    def forward(self):
        if self.tp == 4:
            me = self.me
            hops = self.hops()
            for k in (1, 2):
                self.copy(self.region(me ^ k), k - 1, me ^ k).wait_recv()
                hops[k - 1].start()

    def finish(self):
        me, tp = self.me, self.tp
        if tp == 4:
            self.copy(self.half(me ^ 3, 0), 2, me ^ 2).wait_recv()
            self.copy(self.half(me ^ 3, 1), 3, me ^ 1).wait_recv()
        else:
            for k in range(1, tp):
                owner = lax.rem(me + tp - k, tp)
                self.copy(self.region(owner), k - 1, owner).wait_recv()

    def drain(self):
        for copy in self.outs() + (self.hops() if self.tp == 4 else []):
            copy.wait_send()


def kernel(
    ep, tp,
    q_hbm, k_hbm, v_hbm, g_hbm, ld_ref, tab_hbm, rows_hbm, gain_ref, routes_ref, rw_ref,
    wo_hbm, wg_hbm, wu_hbm, wd_hbm,
    mix_hbm, moe_hbm,
    q_ref, k_ref, v_ref, g_ref, tab, rows_ref, turn,
    wo, wg, wu, wd, normed, p0, p1, og, x, h, eo, ret, ho, state, landed, excl,
    rq, inside, cums, pack, narrow, mix_out, moe_out,
    w_sem, z_send, z_recv, f_send, f_recv, h_send, h_recv, r_send, r_recv, m_send, m_recv,
    s_send, s_recv, o_sem,
):

    e, t = lax.axis_index("ep"), lax.axis_index("tp")
    rows, d = rows_ref.shape
    cap = 2 * rows // ep
    dq = d // tp
    ff = wd.shape[0]
    fq = ff // tp
    heads = ld_ref.shape[0]
    hd = q_ref.shape[1] // heads
    blocks = rows // BLOCK
    g = ep // 4
    units = chunk_units(ep)
    tile = min(256, fq)
    pieces = 2 if fq >= 512 else 1
    piece = fq // pieces
    core, chip, chips = lax.rem(e, 2), e // 2, ep // 2

    barrier = pltpu.get_barrier_semaphore()

    def greet_ep(off):
        pl.semaphore_signal(barrier, inc=1, device_id={"ep": e ^ off}, device_id_type=MESH)

    each(1, ep, greet_ep)
    for k in range(1, tp):
        pl.semaphore_signal(
            barrier, inc=1, device_id={"tp": lax.rem(t + k, tp)}, device_id_type=MESH
        )

    parts = 2
    step_rows = rows // parts
    part_at = [slice(i * step_rows, (i + 1) * step_rows) for i in range(parts)]
    row_loads = [
        pltpu.make_async_copy(rows_hbm.at[at, :], rows_ref.at[at, :], w_sem.at[7 + i])
        for i, at in enumerate(part_at)
    ]
    loads = [
        pltpu.make_async_copy(src, dst, w_sem.at[i])
        for i, (src, dst) in enumerate(
            (
                (wd_hbm.at[0], wd), (wo_hbm, wo),
                (q_hbm, q_ref), (k_hbm, k_ref), (v_hbm, v_ref), (g_hbm, g_ref), (tab_hbm, tab),
            )
        )
    ]
    weight_loads = [
        [
            pltpu.make_async_copy(
                src.at[0, :, j * piece : (j + 1) * piece], dst.at[:, j * piece : (j + 1) * piece],
                w_sem.at[9 + 2 * j + i],
            )
            for i, (src, dst) in enumerate(((wg_hbm, wg), (wu_hbm, wu)))
        ]
        for j in range(pieces)
    ]
    for load in row_loads + sum(weight_loads, []):
        load.start()

    routes = [routes_ref[k : k + 1, :] for k in range(2)]
    experts = lax.broadcasted_iota(jnp.int32, (max(8, ep), rows), 0)
    hot = [(experts == routes[k]).astype(F32) for k in range(2)]
    before = (
        lax.broadcasted_iota(jnp.int32, (rows, rows), 0)
        < lax.broadcasted_iota(jnp.int32, (rows, rows), 1)
    ).astype(F32).astype(BF16)
    rank = dot((hot[0] + hot[1]).astype(BF16), before)
    targets = [
        routes[k] * cap + jnp.sum(rank * hot[k], axis=0, keepdims=True).astype(jnp.int32)
        for k in range(2)
    ]

    for i, at in enumerate(part_at):
        row_loads[i].wait()
        squares = None
        for c in range(d // 128):
            val = rows_ref[at, c * 128 : (c + 1) * 128].astype(F32)
            squares = val * val if squares is None else squares + val * val
        scale = lax.rsqrt(jnp.sum(squares, axis=-1, keepdims=True) / d + 1e-06)
        for c in range(d // 128):
            cols = slice(c * 128, (c + 1) * 128)
            val = rows_ref[at, cols].astype(F32)
            normed[at, cols] = (val * scale * gain_ref[c : c + 1, :].astype(F32)).astype(BF16)

    def unit_at(low, size):
        return span((e // size) ^ (low // size), size * cap)

    def pick(low, size):
        slot = lax.broadcasted_iota(jnp.int32, (size * cap, rows), 0) + (
            (e // size) ^ (low // size)
        ) * (size * cap)
        return ((slot == targets[0]) | (slot == targets[1])).astype(F32).astype(BF16)

    def group(low, size, start, width):
        chosen = pick(low, size)
        wide = min(256, width)
        for c in range(width // wide):
            cols = pl.ds(pl.multiple_of(start + c * wide, wide), wide)
            og[unit_at(low, size), cols] = dot(chosen, normed[:, cols]).astype(BF16)

    group(0, g, 0, d)
    group(2 * g, g, t * dq, dq)
    pl.semaphore_wait(barrier, ep - 1 + tp - 1)

    def z_copy(off, here, whole):
        other = e ^ off
        land = span(other if here else e, cap)
        if whole:
            src, dst = og.at[span(other, cap), :], x.at[land, :]
        else:
            src, dst = og.at[span(other, cap), span(t, dq)], x.at[land, span(t, dq)]
        return pltpu.make_async_remote_copy(
            src_ref=src, dst_ref=dst, send_sem=z_send.at[other],
            recv_sem=z_recv.at[other if here else e],
            device_id={"ep": other}, device_id_type=MESH,
        )

    slim = [(2, g), (2 * g, 3 * g)]
    full = [(g, 2 * g), (3 * g, 4 * g)]

    def z_start(low, high, whole):
        each(low, high, lambda off: z_copy(off, False, whole).start())

    z_start(1, 2, True)
    for low, high in slim:
        z_start(low, high, False)
    for load in loads[2:7] + loads[0:2]:
        load.start()
    x[span(e, cap), :] = og[span(e, cap), :]
    for low, high in full:
        group(low, high - low, 0, d)

    @pl.when(core == 0)
    def _():
        z_start(*full[0], True)


    def row_gather(off):
        other = e ^ off
        start = other * cap

        def half(owner, k):
            return x.at[
                pl.ds(pl.multiple_of(start + k * (cap // 2), cap // 2), cap // 2), span(owner, dq)
            ]

        return Gather(
            tp, lambda owner: x.at[span(other, cap), span(owner, dq)], half,
            lambda slot: f_send.at[other, slot], lambda slot: f_recv.at[other, slot],
        )

    def hid_gather(u, j):
        low, size = units[u]
        count = size * cap
        base = ((e // size) ^ (low // size)) * count

        def cols(owner):
            return pl.ds(pl.multiple_of(owner * fq + j * piece, piece), piece)

        return Gather(
            tp,
            lambda owner: h.at[pl.ds(pl.multiple_of(base, count), count), cols(owner)],
            lambda owner, k: h.at[
                pl.ds(pl.multiple_of(base + k * (count // 2), count // 2), count // 2), cols(owner)
            ],
            lambda slot: h_send.at[u * pieces + j, slot],
            lambda slot: h_recv.at[u * pieces + j, slot],
        )

    half_rows = rows // 2

    def mix_gather(b):
        def at(low, size):
            return slice(b * half_rows + low, b * half_rows + low + size)

        return Gather(
            tp, lambda owner: ho.at[at(0, half_rows), span(owner, heads * hd)],
            lambda owner, k: ho.at[
                at(k * (half_rows // 2), half_rows // 2), span(owner, heads * hd)
            ],
            lambda slot: m_send.at[b, slot], lambda slot: m_recv.at[b, slot],
        )

    def take_rows(off):
        z_copy(off, True, False).wait_recv()
        row_gather(off).start()

    def hidden_piece(u, j):
        at = unit_at(*units[u])

        @pl.loop(0, piece // tile)
        def _(i):
            cols = pl.ds(pl.multiple_of(j * piece + i * tile, tile), tile)
            held = x[at, :]
            gate = dot(held, wg[:, cols])
            up = dot(held, wu[:, cols])
            hid = (gate / (1.0 + jnp.exp(-gate)) * up).astype(BF16)
            h[at, pl.ds(pl.multiple_of(t * fq + j * piece + i * tile, tile), tile)] = hid

        hid_gather(u, j).start()

    def back_copy(off, here):
        other = e ^ off
        return pltpu.make_async_remote_copy(
            src_ref=eo.at[span(other, cap), :], dst_ref=ret.at[span(other if here else e, cap), :],
            send_sem=r_send.at[other], recv_sem=r_recv.at[other if here else e],
            device_id={"ep": other}, device_id_type=MESH,
        )

    out_tile = min(256, dq)

    def down(u):
        for j in range(pieces):
            hid_gather(u, j).finish()
        low, size = units[u]
        at = unit_at(low, size)

        @pl.loop(0, dq // out_tile)
        def _(i):
            cols = pl.ds(pl.multiple_of(i * out_tile, out_tile), out_tile)
            eo[at, cols] = dot(h[at, :], wd[:, cols]).astype(BF16)

        each(max(1, low), low + size, lambda off: back_copy(off, False).start())
        if low == 0:
            ret[span(e, cap), :] = eo[span(e, cap), :]

    def forward(u, j):
        hid_gather(u, j).forward()

    row_i = lax.broadcasted_iota(jnp.int32, (BLOCK, BLOCK), 0)
    col_j = lax.broadcasted_iota(jnp.int32, (BLOCK, BLOCK), 1)
    causal = row_i >= col_j
    lower = causal.astype(F32)
    factor = hd ** (-0.5)
    decay_at = heads * hd

    def retention_local():
        pack[...] = jnp.zeros_like(pack)
        pack[0:1, :] = targets[0].astype(F32)
        pack[1:2, :] = targets[1].astype(F32)
        pack[2:4, :] = rw_ref[...]
        pack[4 : 4 + heads, :] = ld_ref[...]
        for b in range(rows // 128):
            narrow[b * 128 : (b + 1) * 128, :] = pack[:, b * 128 : (b + 1) * 128].T
        lanes = lax.broadcasted_iota(jnp.int32, (rows, ep * cap), 1)
        for k, ref in ((0, p0), (1, p1)):
            ref[...] = (lanes == narrow[:, k : k + 1].astype(jnp.int32)).astype(F32).astype(BF16)
        for load in loads[2:7]:
            load.wait()
        here_cos = tab[pl.ds(2 * rows + e, 1), :]
        here_sin = tab[pl.ds(2 * rows + ep + e, 1), :]
        sign = jnp.where(lax.broadcasted_iota(jnp.int32, (BLOCK, hd), 1) < hd // 2, -1.0, 1.0)
        for b in range(blocks):
            at = slice(b * BLOCK, (b + 1) * BLOCK)
            cos, sin = tab[at, :], tab[slice(rows + b * BLOCK, rows + (b + 1) * BLOCK), :]
            turn[0, at, :] = cos * here_cos - sin * here_sin
            turn[1, at, :] = (sin * here_cos + cos * here_sin) * sign
            cums[at, :] = lax.dot_general(
                lower, narrow[at, :], (((1,), (0,)), ((), ())),
                preferred_element_type=F32, precision=lax.Precision.HIGHEST,
            )
        for n in range(heads):
            cols = slice(n * hd, (n + 1) * hd)
            total = None
            gone = None
            for b in range(blocks):
                at = slice(b * BLOCK, (b + 1) * BLOCK)
                cos, sin = turn[0, at, :], turn[1, at, :]

                def turned(ref):
                    val = ref[at, cols].astype(F32)
                    return val * cos + pltpu.roll(val, hd // 2, 1) * sin

                qb = turned(q_ref).astype(BF16)
                kb = (turned(k_ref) * factor).astype(BF16)
                vb = v_ref[at, cols]
                rq[at, cols] = qb
                cum = jnp.broadcast_to(cums[at, 4 + n : 5 + n], (BLOCK, BLOCK))
                spread = cum - cum.T
                weight = jnp.where(causal, jnp.exp(jnp.where(causal, spread, 0.0)), 0.0)
                scores = dot(qb, kb, ((1,), (1,)))
                inside[at, cols] = dot((scores * weight).astype(BF16), vb)
                ending = cum[BLOCK - 1 : BLOCK, :]
                k_hi, k_lo = split(kb.astype(F32) * jnp.exp(ending - cum))
                update = dot(k_hi, vb, ((0,), (0,))) + dot(k_lo, vb, ((0,), (0,)))
                if b == 0:
                    total, gone = update, ending
                else:
                    total = jnp.exp(ending) * total + update
                    gone = gone + ending
                if b < blocks - 1:
                    excl[1 + b, n * hd : (n + 1) * hd, :] = total
            state[0, n * hd : (n + 1) * hd, :] = total
            state[0, decay_at + n : decay_at + n + 1, :] = jnp.exp(gone)
        excl[0, :decay_at, :] = jnp.zeros((decay_at, hd), F32)

    def up_copy():
        return pltpu.make_async_remote_copy(
            src_ref=state.at[0], dst_ref=landed.at[0], send_sem=s_send.at[0],
            recv_sem=s_recv.at[0], device_id={"ep": e ^ 1}, device_id_type=MESH,
        )

    def next_copy():
        return pltpu.make_async_remote_copy(
            src_ref=state.at[1, :decay_at, :], dst_ref=landed.at[1, :decay_at, :],
            send_sem=s_send.at[1], recv_sem=s_recv.at[1],
            device_id={"ep": lax.rem(e + 2, ep)}, device_id_type=MESH,
        )

    def down_copy():
        part = landed.at[1, :decay_at, :]
        return pltpu.make_async_remote_copy(
            src_ref=part, dst_ref=part, send_sem=s_send.at[2], recv_sem=s_recv.at[2],
            device_id={"ep": e ^ 1}, device_id_type=MESH,
        )

    def decays(n):
        at = slice(decay_at + n, decay_at + n + 1)
        return landed[0, at, :], state[0, at, :]

    def scan_open():
        @pl.when(core == 1)
        def _():
            up_copy().wait_recv()
            for n in range(heads):
                at = slice(n * hd, (n + 1) * hd)
                mine = decays(n)[1]
                state[1, at, :] = mine * landed[0, at, :] + state[0, at, :]
                excl[0, at, :] = landed[0, at, :]

        if chips > 1:

            @pl.when((core == 1) & (chip == 0))
            def _():
                next_copy().start()

    def scan_pass(turn_of):
        @pl.when((core == 1) & turn_of)
        def _():
            next_copy().wait_recv()
            down_copy().start()
            for n in range(heads):
                at = slice(n * hd, (n + 1) * hd)
                first, mine = decays(n)
                came = landed[1, at, :]
                state[1, at, :] = (first * mine) * came + state[1, at, :]
                excl[0, at, :] = first * came + excl[0, at, :]

        @pl.when((core == 1) & turn_of & (chip < chips - 1))
        def _():
            next_copy().start()

    def scan_close():
        @pl.when((core == 0) & (chip > 0))
        def _():
            down_copy().wait_recv()
            excl[0, :decay_at, :] = landed[1, :decay_at, :]

    def retention_close():
        for n in range(heads):
            cols = slice(n * hd, (n + 1) * hd)
            sat = slice(n * hd, (n + 1) * hd)
            entering = excl[0, sat, :]
            gone = None
            for b in range(blocks):
                at = slice(b * BLOCK, (b + 1) * BLOCK)
                cum = jnp.broadcast_to(cums[at, 4 + n : 5 + n], (BLOCK, hd))
                held = entering if b == 0 else jnp.exp(gone) * entering + excl[b, sat, :]
                hi, lo = split(held)
                qb = rq[at, cols]
                retained = inside[at, cols] + (dot(qb, hi) + dot(qb, lo)) * jnp.exp(cum)
                scale = lax.rsqrt(jnp.mean(retained * retained, axis=-1, keepdims=True) + 1e-05)
                gate = g_ref[at, cols].astype(F32)
                out = (retained * scale * (gate / (1.0 + jnp.exp(-gate)))).astype(BF16)
                ho[at, pl.ds(pl.multiple_of(t * heads * hd + n * hd, hd), hd)] = out
                ending = cum[BLOCK - 1 : BLOCK, :]
                gone = ending if gone is None else gone + ending

    for load in weight_loads[0]:
        load.wait()
    z_copy(1, True, True).wait_recv()
    each(2, g, take_rows)
    each(2, g, lambda off: row_gather(off).forward())
    each(2, g, lambda off: row_gather(off).finish())
    hidden_piece(0, 0)
    retention_local()

    @pl.when(core == 0)
    def _():
        up_copy().start()

    for j in range(1, pieces):
        for load in weight_loads[j]:
            load.wait()
        hidden_piece(0, j)
    scan_open()
    last = full[1][1] - (full[1][1] - full[1][0]) // 2

    @pl.when(core == 1)
    def _():
        z_start(*full[0], True)
        z_start(full[1][0], last, True)

    @pl.when(core == 0)
    def _():
        z_start(*full[1], True)


    each(2 * g, 3 * g, take_rows)
    each(2 * g, 3 * g, lambda off: row_gather(off).forward())
    for j in range(pieces):
        forward(0, j)
    scan_pass(chip == 1)

    @pl.when(core == 1)
    def _():
        z_start(last, full[1][1], True)

    each(2 * g, 3 * g, lambda off: row_gather(off).finish())
    for j in range(pieces):
        hidden_piece(1, j)

    each(g, 2 * g, lambda off: z_copy(off, True, True).wait_recv())
    for j in range(pieces):
        hidden_piece(2, j)
    loads[0].wait()
    down(0)
    forward(1, 0)
    scan_pass(chip == 2)
    for j in range(1, pieces):
        forward(1, j)
    forward(2, 0)

    def last_rows(u):
        low, size = units[u]
        each(low, low + size, lambda off: z_copy(off, True, True).wait_recv())
        for j in range(pieces):
            hidden_piece(u, j)

    last_rows(3)
    for j in range(1, pieces):
        forward(2, j)
    scan_pass(chip > 2)
    scan_close()
    retention_close()
    mix_gather(0).start()
    last_rows(4)
    down(1)
    for j in range(pieces):
        forward(3, j)
    down(2)
    mix_gather(0).forward()
    for j in range(pieces):
        forward(4, j)
    mix_gather(1).start()
    down(3)
    down(4)
    mix_gather(1).forward()
    loads[1].wait()

    for b in range(2):
        mix_gather(b).finish()

    @pl.loop(0, dq // out_tile)
    def _(i):
        cols = pl.ds(pl.multiple_of(i * out_tile, out_tile), out_tile)
        mix_out[:, cols] = dot(ho[...], wo[:, cols]).astype(BF16)

    mix_write = pltpu.make_async_copy(mix_out, mix_hbm, o_sem.at[0])
    mix_write.start()
    each(1, ep, lambda off: back_copy(off, True).wait_recv())

    @pl.loop(0, dq // out_tile)
    def _(i):
        cols = pl.ds(pl.multiple_of(i * out_tile, out_tile), out_tile)
        came = ret[:, cols]
        moe_out[:, cols] = (
            dot(p0[...], came) * narrow[:, 2:3] + dot(p1[...], came) * narrow[:, 3:4]
        ).astype(BF16)

    moe_write = pltpu.make_async_copy(moe_out, moe_hbm, o_sem.at[1])
    moe_write.start()

    def drain(low, high, whole):
        each(low, high, lambda off: z_copy(off, False, whole).wait_send())

    drain(1, 2, True)
    for low, high in slim:
        drain(low, high, False)
        each(low, high, lambda off: row_gather(off).drain())
    for low, high in full:
        drain(low, high, True)
    each(1, ep, lambda off: back_copy(off, False).wait_send())
    for u in range(len(units)):
        for j in range(pieces):
            hid_gather(u, j).drain()
    for b in range(2):
        mix_gather(b).drain()

    @pl.when(core == 0)
    def _():
        up_copy().wait_send()

    @pl.when((core == 1) & (chip < chips - 1))
    def _():
        next_copy().wait_send()

    @pl.when((core == 1) & (chip > 0))
    def _():
        down_copy().wait_send()

    mix_write.wait()
    moe_write.wait()


def turn_table(ep, rows, hd):
    half = hd // 2
    inverse = np.tile(10000.0 ** (-np.arange(half) / half), 2)
    near = np.arange(rows)[:, None] * inverse[None, :]
    far = (np.arange(ep) * rows)[:, None] * inverse[None, :]
    parts = [np.cos(near), np.sin(near), np.cos(far), np.sin(far)]
    return np.concatenate(parts).astype(np.float32)


def on_device(
    ep, tp,
    queries, keys, values, gates, log_decay, out_weight, moe_rows, moe_gain, routes,
    route_weights, gate_proj, up_proj, down_proj,
):
    rows, d = moe_rows.shape
    heads = log_decay.shape[1]
    width = queries.shape[1]
    hd = width // heads
    cap = 2 * rows // ep
    dq = d // tp
    fq = gate_proj.shape[2]
    ff = down_proj.shape[1]
    slots = max(4, tp - 1)
    pieces = len(chunk_units(ep)) * 2
    blocks = rows // BLOCK
    srows = heads * hd + 8 * ((heads + 7) // 8)
    vmem = pl.BlockSpec(memory_space=pltpu.VMEM)
    hbm = pl.BlockSpec(memory_space=pl.ANY)
    dma = pltpu.SemaphoreType.DMA
    out = jax.ShapeDtypeStruct((rows, dq), BF16)
    table = jnp.asarray(turn_table(ep, rows, hd))
    return pl.pallas_call(
        functools.partial(kernel, ep, tp),
        out_shape=(out, out),
        in_specs=[hbm] * 4 + [vmem, hbm, hbm] + [vmem] * 3 + [hbm] * 4,
        out_specs=(hbm, hbm),
        scratch_shapes=[
            pltpu.VMEM((rows, width), BF16),
            pltpu.VMEM((rows, width), BF16),
            pltpu.VMEM((rows, width), BF16),
            pltpu.VMEM((rows, width), BF16),
            pltpu.VMEM(table.shape, F32),
            pltpu.VMEM((rows, d), BF16),
            pltpu.VMEM((2, rows, hd), F32),
            pltpu.VMEM(out_weight.shape, BF16),
            pltpu.VMEM((d, fq), BF16),
            pltpu.VMEM((d, fq), BF16),
            pltpu.VMEM((ff, dq), BF16),
            pltpu.VMEM((rows, d), BF16),
            pltpu.VMEM((rows, ep * cap), BF16),
            pltpu.VMEM((rows, ep * cap), BF16),
            pltpu.VMEM((ep * cap, d), BF16),
            pltpu.VMEM((ep * cap, d), BF16),
            pltpu.VMEM((ep * cap, ff), BF16),
            pltpu.VMEM((ep * cap, dq), BF16),
            pltpu.VMEM((ep * cap, dq), BF16),
            pltpu.VMEM((rows, width * tp), BF16),
            pltpu.VMEM((2, srows, hd), F32),
            pltpu.VMEM((2, srows, hd), F32),
            pltpu.VMEM((blocks, srows, hd), F32),
            pltpu.VMEM((rows, width), BF16),
            pltpu.VMEM((rows, width), F32),
            pltpu.VMEM((rows, 128), F32),
            pltpu.VMEM((128, rows), F32),
            pltpu.VMEM((rows, 128), F32),
            pltpu.VMEM((rows, dq), BF16),
            pltpu.VMEM((rows, dq), BF16),
            dma((13,)),
            dma((ep,)), dma((ep,)),
            dma((ep, slots)), dma((ep, slots)),
            dma((pieces, slots)), dma((pieces, slots)),
            dma((ep,)), dma((ep,)),
            dma((2, slots)), dma((2, slots)),
            dma((3,)), dma((3,)),
            dma((2,)),
        ],
        compiler_params=pltpu.CompilerParams(
            collective_id=0, has_side_effects=True, vmem_limit_bytes=60 * 1024 * 1024
        ),
    )(
        queries, keys, values, gates, log_decay.T, table, moe_rows, moe_gain.reshape(-1, 128),
        routes.T, route_weights.T, out_weight, gate_proj, up_proj, down_proj,
    )


def solution(mesh):
    placed = (
        P("ep", "tp"), P("ep", "tp"), P("ep", "tp"), P("ep", "tp"), P("ep", "tp"),
        P(None, "tp"), P("ep", None), P(), P("ep", None), P("ep", None),
        P("ep", None, "tp"), P("ep", None, "tp"), P("ep", None, "tp"),
    )
    return jax.shard_map(
        functools.partial(on_device, mesh.shape["ep"], mesh.shape["tp"]),
        mesh=mesh, in_specs=placed, out_specs=(P("ep", "tp"), P("ep", "tp")), check_vma=False,
    )
```

time: 90.3 us -> 68.8 us (0.76)
  Pallas kernels: 84.3 us -> 64.6 us
  other arithmetic: 1.26 us -> 0 us
    pallas_call x1, Pallas kernels: 84.3 us -> 64.6 us  [on_device(): pl.pallas_call(functools.partial(kernel, ep, tp), out_shape=(out, out), i...]
    mul x1 -> x0, other arithmetic: 1.24 us -> none  [on_device(): cos, sin = (jnp.cos(angles), jnp.sin(angles) * sign[None, :])]
where the time goes in v1:
time: 68.8 us; the launch traced here: 68.6 us
  Pallas kernels  64.6 us (94%)
  local copies, waits for them, and re-layouts  3.34 us (5%)
    pallas_call x1, Pallas kernels, on_device(): pl.pallas_call(functools.partial(kernel, ep, tp), out_shape=(out, out), i...  64.6 us
    unnamed x2, local copies, waits for them, and re-layouts  3.34 us

profile of v1, /device:TPU:0, one launch (start us, length us, event | category | flops | bytes accessed | tf_op | source)
XLA Modules:
  0.0 68.6 jit_solution(13907685774143220829)
XLA Ops:
  0.6 64.6 %shard_map.149 = (bf16[256,512]{1,0:T(8,128)(2,1)}, bf16[256,512]{1,0:T(8,128)(2,1)}) custom-call(bf16[256,512]{1,0:T(8,128)(2,1)} %q_hbm.1, bf16[256,512]{1,0:T(8,128)(2,1)} %k_hbm.1, bf16[256,512]{1,0:T(8,128)(2,1)} %v_hbm.1, bf16[256,512]{1,0:T(8,128)(2,1)} %g_hbm.1, f32[4,256]{1,0:T(4,128)} %bitcast.4, f32[528,128]{1,0:T(8,128)} %constant.2.clone.tab_hbm, ...), custom_call_target="tpu_custom_call" | custom-call | tf_op jit(solution)/shard_map/pallas_call | solution.py:652
  65.2 1.7 %copy.18 = bf16[256,512]{1,0:T(8,128)(2,1)} copy(bf16[256,512]{1,0:T(8,128)(2,1)} %get-tuple-element.4) | data formatting | bytes 524288
  66.9 1.7 %copy.19 = bf16[256,512]{1,0:T(8,128)(2,1)} copy(bf16[256,512]{1,0:T(8,128)(2,1)} %get-tuple-element.5) | data formatting | bytes 524288

commit v2 on v1

--- a/solution.py
+++ b/solution.py
@@ -96,14 +96,14 @@
 
 def kernel(
     ep, tp,
-    q_hbm, k_hbm, v_hbm, g_hbm, ld_ref, tab_hbm, rows_hbm, gain_ref, routes_ref, rw_ref,
+    q_hbm, k_hbm, v_hbm, g_hbm, ld_hbm, tab_hbm, rows_hbm, gain_hbm, routes_hbm, rw_hbm,
     wo_hbm, wg_hbm, wu_hbm, wd_hbm,
-    mix_hbm, moe_hbm,
-    q_ref, k_ref, v_ref, g_ref, tab, rows_ref, turn,
+    out_ref,
+    ld_ref, gain_ref, routes_ref, rw_ref, q_ref, k_ref, v_ref, g_ref, tab, rows_ref, turn,
     wo, wg, wu, wd, normed, p0, p1, og, x, h, eo, ret, ho, state, landed, excl,
-    rq, inside, cums, pack, narrow, mix_out, moe_out,
+    rq, inside, cums, pack, narrow,
     w_sem, z_send, z_recv, f_send, f_recv, h_send, h_recv, r_send, r_recv, m_send, m_recv,
-    s_send, s_recv, o_sem,
+    s_send, s_recv,
 ):
 
     e, t = lax.axis_index("ep"), lax.axis_index("tp")
@@ -159,9 +159,18 @@
         ]
         for j in range(pieces)
     ]
-    for load in row_loads + sum(weight_loads, []):
+    small_loads = [
+        pltpu.make_async_copy(src, dst, w_sem.at[13 + i])
+        for i, (src, dst) in enumerate(
+            (
+                (routes_hbm, routes_ref), (gain_hbm, gain_ref), (ld_hbm, ld_ref), (rw_hbm, rw_ref),
+            )
+        )
+    ]
+    for load in row_loads + small_loads + sum(weight_loads, []):
         load.start()
 
+    small_loads[0].wait()
     routes = [routes_ref[k : k + 1, :] for k in range(2)]
     experts = lax.broadcasted_iota(jnp.int32, (max(8, ep), rows), 0)
     hot = [(experts == routes[k]).astype(F32) for k in range(2)]
@@ -175,6 +184,7 @@
         for k in range(2)
     ]
 
+    small_loads[1].wait()
     for i, at in enumerate(part_at):
         row_loads[i].wait()
         squares = None
@@ -340,6 +350,8 @@
     decay_at = heads * hd
 
     def retention_local():
+        small_loads[2].wait()
+        small_loads[3].wait()
         pack[...] = jnp.zeros_like(pack)
         pack[0:1, :] = targets[0].astype(F32)
         pack[1:2, :] = targets[1].astype(F32)
@@ -569,22 +581,18 @@
     @pl.loop(0, dq // out_tile)
     def _(i):
         cols = pl.ds(pl.multiple_of(i * out_tile, out_tile), out_tile)
-        mix_out[:, cols] = dot(ho[...], wo[:, cols]).astype(BF16)
-
-    mix_write = pltpu.make_async_copy(mix_out, mix_hbm, o_sem.at[0])
-    mix_write.start()
+        out_ref[0, :, cols] = dot(ho[...], wo[:, cols]).astype(BF16)
+
     each(1, ep, lambda off: back_copy(off, True).wait_recv())
 
     @pl.loop(0, dq // out_tile)
     def _(i):
         cols = pl.ds(pl.multiple_of(i * out_tile, out_tile), out_tile)
         came = ret[:, cols]
-        moe_out[:, cols] = (
+        out_ref[1, :, cols] = (
             dot(p0[...], came) * narrow[:, 2:3] + dot(p1[...], came) * narrow[:, 3:4]
         ).astype(BF16)
 
-    moe_write = pltpu.make_async_copy(moe_out, moe_hbm, o_sem.at[1])
-    moe_write.start()
 
     def drain(low, high, whole):
         each(low, high, lambda off: z_copy(off, False, whole).wait_send())
@@ -613,9 +621,6 @@
     @pl.when((core == 1) & (chip > 0))
     def _():
         down_copy().wait_send()
-
-    mix_write.wait()
-    moe_write.wait()
 
 
 def turn_table(ep, rows, hd):
@@ -645,16 +650,25 @@
     blocks = rows // BLOCK
     srows = heads * hd + 8 * ((heads + 7) // 8)
     vmem = pl.BlockSpec(memory_space=pltpu.VMEM)
-    hbm = pl.BlockSpec(memory_space=pl.ANY)
     dma = pltpu.SemaphoreType.DMA
-    out = jax.ShapeDtypeStruct((rows, dq), BF16)
     table = jnp.asarray(turn_table(ep, rows, hd))
-    return pl.pallas_call(
+    operands = [
+        pltpu.with_memory_space_constraint(operand, pltpu.HBM)
+        for operand in (
+            queries, keys, values, gates, log_decay.T, table, moe_rows, moe_gain.reshape(-1, 128),
+            routes.T, route_weights.T, out_weight, gate_proj, up_proj, down_proj,
+        )
+    ]
+    both = pl.pallas_call(
         functools.partial(kernel, ep, tp),
-        out_shape=(out, out),
-        in_specs=[hbm] * 4 + [vmem, hbm, hbm] + [vmem] * 3 + [hbm] * 4,
-        out_specs=(hbm, hbm),
+        out_shape=jax.ShapeDtypeStruct((2, rows, dq), BF16),
+        in_specs=[pl.BlockSpec(memory_space=pltpu.HBM)] * 14,
+        out_specs=vmem,
         scratch_shapes=[
+            pltpu.VMEM((heads, rows), F32),
+            pltpu.VMEM((d // 128, 128), BF16),
+            pltpu.VMEM((2, rows), jnp.int32),
+            pltpu.VMEM((2, rows), F32),
             pltpu.VMEM((rows, width), BF16),
             pltpu.VMEM((rows, width), BF16),
             pltpu.VMEM((rows, width), BF16),
@@ -683,24 +697,19 @@
             pltpu.VMEM((rows, 128), F32),
             pltpu.VMEM((128, rows), F32),
             pltpu.VMEM((rows, 128), F32),
-            pltpu.VMEM((rows, dq), BF16),
-            pltpu.VMEM((rows, dq), BF16),
-            dma((13,)),
+            dma((17,)),
             dma((ep,)), dma((ep,)),
             dma((ep, slots)), dma((ep, slots)),
             dma((pieces, slots)), dma((pieces, slots)),
             dma((ep,)), dma((ep,)),
             dma((2, slots)), dma((2, slots)),
             dma((3,)), dma((3,)),
-            dma((2,)),
         ],
         compiler_params=pltpu.CompilerParams(
-            collective_id=0, has_side_effects=True, vmem_limit_bytes=60 * 1024 * 1024
+            collective_id=0, has_side_effects=True, vmem_limit_bytes=44 * 1024 * 1024
         ),
-    )(
-        queries, keys, values, gates, log_decay.T, table, moe_rows, moe_gain.reshape(-1, 128),
-        routes.T, route_weights.T, out_weight, gate_proj, up_proj, down_proj,
-    )
+    )(*operands)
+    return both[0], both[1]
 
 
 def solution(mesh):

time: 68.8 us -> 65 us (0.945)
  local copies, waits for them, and re-layouts: 3.34 us -> 0.82 us
  Pallas kernels: 64.6 us -> 63.3 us
    unnamed x2 -> x0, local copies, waits for them, and re-layouts: 3.34 us -> none
    pallas_call x1, Pallas kernels: 64.6 us -> 63.3 us  [on_device(): pl.pallas_call(functools.partial(kernel, ep, tp), out_shape=jax.ShapeDtyp...]
    squeeze x0 -> x1, local copies, waits for them, and re-layouts: none -> 0.82 us  [on_device(): return (both[0], both[1])]
where the time goes in v2:
time: 65 us; the launch traced here: 64.8 us
  Pallas kernels  63.3 us (97%)
  local copies, waits for them, and re-layouts  0.82 us (1%)
    pallas_call x1, Pallas kernels, on_device(): pl.pallas_call(functools.partial(kernel, ep, tp), out_shape=jax.ShapeDtyp...  63.3 us

profile of v2, /device:TPU:0, one launch (start us, length us, event | category | flops | bytes accessed | tf_op | source)
XLA Modules:
  0.0 64.8 jit_solution(302948463217465957)
XLA Ops:
  0.6 63.3 %shard_map.149 = bf16[2,256,512]{2,1,0:T(8,128)(2,1)S(1)} custom-call(bf16[256,512]{1,0:T(8,128)(2,1)} %q_hbm.1, bf16[256,512]{1,0:T(8,128)(2,1)} %k_hbm.1, bf16[256,512]{1,0:T(8,128)(2,1)} %v_hbm.1, bf16[256,512]{1,0:T(8,128)(2,1)} %g_hbm.1, f32[4,256]{1,0:T(4,128)} %bitcast.8, f32[528,128]{1,0:T(8,128)} %constant.2.clone.tab_hbm, ...), custom_call_target="tpu_custom_call" | custom-call | tf_op jit(solution)/shard_map/pallas_call | solution.py:662
  64.0 0.8 %slice_bitcast_fusion = (bf16[256,512]{1,0:T(8,128)(2,1)}, bf16[256,512]{1,0:T(8,128)(2,1)}) fusion(bf16[2,256,512]{2,1,0:T(8,128)(2,1)S(1)} %shard_map.149), kind=kLoop, calls=%fused_computation | loop fusion | bytes 1048576 | tf_op jit(solution)/shard_map/squeeze | solution.py:712

commit v3 on v2

--- a/solution.py
+++ b/solution.py
@@ -38,60 +38,48 @@
     return lax.dot_general(a, b, (dims, ((), ())), preferred_element_type=F32)
 
 
-def chunk_units(ep):
-    g = ep // 4
-    return [(0, g), (2 * g, g), (g, g), (3 * g, g // 2), (3 * g + g // 2, g // 2)]
+def plan(ep):
+    q = ep // 8
+    order = ((0, False), (1, False), (4, False), (6, False), (2, True), (5, True), (7, True), (3, True))
+    return [(low * q, q, whole) for low, whole in order]
 
 
 class Gather:
-    def __init__(self, tp, region, half, send, recv):
-        self.tp, self.region, self.half, self.send, self.recv = tp, region, half, send, recv
+    def __init__(self, tp, region, half, send, recv, hop):
+        self.tp, self.region, self.half, self.send = tp, region, half, send
+        self.recv, self.hop = recv, hop
         self.me = lax.axis_index("tp")
 
-    def copy(self, ref, slot, to):
+    def copy(self, ref, recv, to):
         return pltpu.make_async_remote_copy(
-            src_ref=ref, dst_ref=ref, send_sem=self.send(slot), recv_sem=self.recv(slot),
+            src_ref=ref, dst_ref=ref, send_sem=self.send, recv_sem=recv,
             device_id={"tp": to}, device_id_type=MESH,
         )
 
-    def outs(self):
+    def start(self):
         me, tp = self.me, self.tp
         if tp == 4:
-            return [self.copy(self.region(me), k - 1, me ^ k) for k in (1, 2)]
-        return [self.copy(self.region(me), k - 1, lax.rem(me + k, tp)) for k in range(1, tp)]
-
-    def hops(self):
-        me = self.me
-        return [
-            self.copy(self.half(me ^ 1, 0), 2, me ^ 2),
-            self.copy(self.half(me ^ 2, 1), 3, me ^ 1),
-        ]
-
-    def start(self):
-        for copy in self.outs():
-            copy.start()
+            for k in (1, 2):
+                self.copy(self.region(me), self.recv(k - 1), me ^ k).start()
+        else:
+            for k in range(1, tp):
+                self.copy(self.region(me), self.recv(k - 1), lax.rem(me + k, tp)).start()
 
     def forward(self):
         if self.tp == 4:
             me = self.me
-            hops = self.hops()
             for k in (1, 2):
-                self.copy(self.region(me ^ k), k - 1, me ^ k).wait_recv()
-                hops[k - 1].start()
+                self.copy(self.region(me ^ k), self.recv(k - 1), me ^ k).wait_recv()
+                self.copy(self.half(me ^ k, k - 1), self.hop, me ^ (3 - k)).start()
 
     def finish(self):
         me, tp = self.me, self.tp
         if tp == 4:
-            self.copy(self.half(me ^ 3, 0), 2, me ^ 2).wait_recv()
-            self.copy(self.half(me ^ 3, 1), 3, me ^ 1).wait_recv()
+            self.copy(self.region(me ^ 3), self.hop, me ^ 3).wait_recv()
         else:
             for k in range(1, tp):
                 owner = lax.rem(me + tp - k, tp)
-                self.copy(self.region(owner), k - 1, owner).wait_recv()
-
-    def drain(self):
-        for copy in self.outs() + (self.hops() if self.tp == 4 else []):
-            copy.wait_send()
+                self.copy(self.region(owner), self.recv(k - 1), owner).wait_recv()
 
 
 def kernel(
@@ -99,11 +87,10 @@
     q_hbm, k_hbm, v_hbm, g_hbm, ld_hbm, tab_hbm, rows_hbm, gain_hbm, routes_hbm, rw_hbm,
     wo_hbm, wg_hbm, wu_hbm, wd_hbm,
     out_ref,
-    ld_ref, gain_ref, routes_ref, rw_ref, q_ref, k_ref, v_ref, g_ref, tab, rows_ref, turn,
-    wo, wg, wu, wd, normed, p0, p1, og, x, h, eo, ret, ho, state, landed, excl,
+    ld_ref, gain_ref, routes_ref, rw_ref, heads_in, tab, rows_ref, turn,
+    wo, wg, wu, wd, normed, p0, p1, og, x, h, eo, ret, ho, state, landed, passed, excl, partial,
     rq, inside, cums, pack, narrow,
-    w_sem, z_send, z_recv, f_send, f_recv, h_send, h_recv, r_send, r_recv, m_send, m_recv,
-    s_send, s_recv,
+    w_sem, sent, z_recv, f_recv, f_hop, h_recv, h_hop, r_recv, m_recv, m_hop, s_send, s_recv,
 ):
 
     e, t = lax.axis_index("ep"), lax.axis_index("tp")
@@ -113,13 +100,16 @@
     ff = wd.shape[0]
     fq = ff // tp
     heads = ld_ref.shape[0]
-    hd = q_ref.shape[1] // heads
+    hd = heads_in.shape[2] // heads
+    q_ref, k_ref, v_ref, g_ref = [heads_in.at[i] for i in range(4)]
     blocks = rows // BLOCK
     g = ep // 4
-    units = chunk_units(ep)
+    units = plan(ep)
     tile = min(256, fq)
     pieces = 2 if fq >= 512 else 1
     piece = fq // pieces
+    cuts = [(j * piece, piece) for j in range(pieces)]
+    first = [(0, tile), (tile, piece - tile)] * (piece > tile) + cuts[piece > tile :]
     core, chip, chips = lax.rem(e, 2), e // 2, ep // 2
 
     barrier = pltpu.get_barrier_semaphore()
@@ -137,30 +127,33 @@
     step_rows = rows // parts
     part_at = [slice(i * step_rows, (i + 1) * step_rows) for i in range(parts)]
     row_loads = [
-        pltpu.make_async_copy(rows_hbm.at[at, :], rows_ref.at[at, :], w_sem.at[7 + i])
+        pltpu.make_async_copy(rows_hbm.at[at, :], rows_ref.at[at, :], w_sem.at[4 + i])
         for i, at in enumerate(part_at)
     ]
     loads = [
         pltpu.make_async_copy(src, dst, w_sem.at[i])
         for i, (src, dst) in enumerate(
             (
-                (wd_hbm.at[0], wd), (wo_hbm, wo),
-                (q_hbm, q_ref), (k_hbm, k_ref), (v_hbm, v_ref), (g_hbm, g_ref), (tab_hbm, tab),
+                (wd_hbm.at[0], wd), (wo_hbm, wo), (tab_hbm, tab),
             )
         )
+    ]
+    head_loads = [
+        pltpu.make_async_copy(src, dst, w_sem.at[3])
+        for src, dst in ((q_hbm, q_ref), (k_hbm, k_ref), (v_hbm, v_ref), (g_hbm, g_ref))
     ]
     weight_loads = [
         [
             pltpu.make_async_copy(
                 src.at[0, :, j * piece : (j + 1) * piece], dst.at[:, j * piece : (j + 1) * piece],
-                w_sem.at[9 + 2 * j + i],
+                w_sem.at[6 + 2 * j + i],
             )
             for i, (src, dst) in enumerate(((wg_hbm, wg), (wu_hbm, wu)))
         ]
         for j in range(pieces)
     ]
     small_loads = [
-        pltpu.make_async_copy(src, dst, w_sem.at[13 + i])
+        pltpu.make_async_copy(src, dst, w_sem.at[10 + i])
         for i, (src, dst) in enumerate(
             (
                 (routes_hbm, routes_ref), (gain_hbm, gain_ref), (ld_hbm, ld_ref), (rw_hbm, rw_ref),
@@ -214,7 +207,8 @@
             og[unit_at(low, size), cols] = dot(chosen, normed[:, cols]).astype(BF16)
 
     group(0, g, 0, d)
-    group(2 * g, g, t * dq, dq)
+    for low, size, whole in units[2:4]:
+        group(low, size, t * dq, dq)
     pl.semaphore_wait(barrier, ep - 1 + tp - 1)
 
     def z_copy(off, here, whole):
@@ -225,34 +219,47 @@
         else:
             src, dst = og.at[span(other, cap), span(t, dq)], x.at[land, span(t, dq)]
         return pltpu.make_async_remote_copy(
-            src_ref=src, dst_ref=dst, send_sem=z_send.at[other],
+            src_ref=src, dst_ref=dst, send_sem=sent.at[0 if whole else 1],
             recv_sem=z_recv.at[other if here else e],
             device_id={"ep": other}, device_id_type=MESH,
         )
 
-    slim = [(2, g), (2 * g, 3 * g)]
-    full = [(g, 2 * g), (3 * g, 4 * g)]
-
-    def z_start(low, high, whole):
+    def offsets(u):
+        low, size, whole = units[u]
+        return max(2, low), max(2, low + size), whole
+
+    def z_start(u):
+        low, high, whole = offsets(u)
         each(low, high, lambda off: z_copy(off, False, whole).start())
 
-    z_start(1, 2, True)
-    for low, high in slim:
-        z_start(low, high, False)
-    for load in loads[2:7] + loads[0:2]:
+    def z_wait(u):
+        low, high, whole = offsets(u)
+        each(low, high, lambda off: z_copy(off, True, whole).wait_recv())
+
+    z_copy(1, False, True).start()
+    for u in range(4):
+        z_start(u)
+    for load in head_loads + loads[2:3] + loads[0:2]:
         load.start()
     x[span(e, cap), :] = og[span(e, cap), :]
-    for low, high in full:
-        group(low, high - low, 0, d)
-
-    @pl.when(core == 0)
-    def _():
-        z_start(*full[0], True)
-
-
-    def row_gather(off):
+    group(*units[4][:2], 0, d)
+    opens = (core == 1) & (chip == 0)
+
+    @pl.when(jnp.logical_not(opens))
+    def _():
+        z_start(4)
+
+
+    slim_at, count = [], 0
+    for u in range(4):
+        low, high, _ = offsets(u)
+        slim_at.append(count - low)
+        count += high - low
+
+    def row_gather(u, off):
         other = e ^ off
         start = other * cap
+        at = slim_at[u] + off
 
         def half(owner, k):
             return x.at[
@@ -261,16 +268,34 @@
 
         return Gather(
             tp, lambda owner: x.at[span(other, cap), span(owner, dq)], half,
-            lambda slot: f_send.at[other, slot], lambda slot: f_recv.at[other, slot],
-        )
-
-    def hid_gather(u, j):
-        low, size = units[u]
+            sent.at[2], lambda slot: f_recv.at[at, slot], f_hop.at[at],
+        )
+
+    def rows_start(u):
+        low, high, _ = offsets(u)
+
+        def take(off):
+            z_copy(off, True, False).wait_recv()
+            row_gather(u, off).start()
+
+        each(low, high, take)
+
+    def rows_forward(u):
+        low, high, _ = offsets(u)
+        each(low, high, lambda off: row_gather(u, off).forward())
+
+    def rows_finish(u):
+        low, high, _ = offsets(u)
+        each(low, high, lambda off: row_gather(u, off).finish())
+
+    def hid_gather(u, number):
+        start, width = (0, fq) if number is None else (first if u in (0, 2) else cuts)[number]
+        low, size, _ = units[u]
         count = size * cap
         base = ((e // size) ^ (low // size)) * count
 
         def cols(owner):
-            return pl.ds(pl.multiple_of(owner * fq + j * piece, piece), piece)
+            return pl.ds(pl.multiple_of(owner * fq + start, tile), width)
 
         return Gather(
             tp,
@@ -278,9 +303,15 @@
             lambda owner, k: h.at[
                 pl.ds(pl.multiple_of(base + k * (count // 2), count // 2), count // 2), cols(owner)
             ],
-            lambda slot: h_send.at[u * pieces + j, slot],
-            lambda slot: h_recv.at[u * pieces + j, slot],
-        )
+            sent.at[3], lambda slot: h_recv.at[u * 3 + number, slot], h_hop.at[u],
+        )
+
+    def hid_finish(u):
+        if tp == 4:
+            hid_gather(u, None).finish()
+        else:
+            for j in range(len(first if u in (0, 2) else cuts)):
+                hid_gather(u, j).finish()
 
     half_rows = rows // 2
 
@@ -293,49 +324,63 @@
             lambda owner, k: ho.at[
                 at(k * (half_rows // 2), half_rows // 2), span(owner, heads * hd)
             ],
-            lambda slot: m_send.at[b, slot], lambda slot: m_recv.at[b, slot],
-        )
-
-    def take_rows(off):
-        z_copy(off, True, False).wait_recv()
-        row_gather(off).start()
+            sent.at[4], lambda slot: m_recv.at[b, slot], m_hop.at[b],
+        )
 
     def hidden_piece(u, j):
-        at = unit_at(*units[u])
-
-        @pl.loop(0, piece // tile)
+        at = unit_at(*units[u][:2])
+        start, width = (first if u in (0, 2) else cuts)[j]
+
+        @pl.loop(0, width // tile)
         def _(i):
-            cols = pl.ds(pl.multiple_of(j * piece + i * tile, tile), tile)
+            cols = pl.ds(pl.multiple_of(start + i * tile, tile), tile)
             held = x[at, :]
             gate = dot(held, wg[:, cols])
             up = dot(held, wu[:, cols])
             hid = (gate / (1.0 + jnp.exp(-gate)) * up).astype(BF16)
-            h[at, pl.ds(pl.multiple_of(t * fq + j * piece + i * tile, tile), tile)] = hid
+            h[at, pl.ds(pl.multiple_of(t * fq + start + i * tile, tile), tile)] = hid
 
         hid_gather(u, j).start()
 
-    def back_copy(off, here):
+    def back_copy(off, cols):
         other = e ^ off
         return pltpu.make_async_remote_copy(
-            src_ref=eo.at[span(other, cap), :], dst_ref=ret.at[span(other if here else e, cap), :],
-            send_sem=r_send.at[other], recv_sem=r_recv.at[other if here else e],
+            src_ref=eo.at[span(other, cap), cols], dst_ref=ret.at[span(e, cap), cols],
+            send_sem=sent.at[5], recv_sem=r_recv.at[0],
             device_id={"ep": other}, device_id_type=MESH,
         )
 
     out_tile = min(256, dq)
 
-    def down(u):
-        for j in range(pieces):
-            hid_gather(u, j).finish()
-        low, size = units[u]
+    def down_early(u):
+        if tp == 4:
+            at = unit_at(*units[u][:2])
+
+            @pl.loop(0, dq // out_tile)
+            def _(i):
+                cols = pl.ds(pl.multiple_of(i * out_tile, out_tile), out_tile)
+                partial[u % 2, :, cols] = sum(
+                    dot(h[at, span(t ^ k, fq)], wd[span(t ^ k, fq), cols]) for k in range(3)
+                )
+
+    def down(u, early=False):
+        hid_finish(u)
+        low, size, _ = units[u]
         at = unit_at(low, size)
 
         @pl.loop(0, dq // out_tile)
         def _(i):
             cols = pl.ds(pl.multiple_of(i * out_tile, out_tile), out_tile)
-            eo[at, cols] = dot(h[at, :], wd[:, cols]).astype(BF16)
-
-        each(max(1, low), low + size, lambda off: back_copy(off, False).start())
+            if early and tp == 4:
+                done = t ^ 3
+                total = partial[u % 2, :, cols] + dot(
+                    h[at, span(done, fq)], wd[span(done, fq), cols]
+                )
+            else:
+                total = dot(h[at, :], wd[:, cols])
+            eo[at, cols] = total.astype(BF16)
+            each(max(1, low), low + size, lambda off: back_copy(off, cols).start())
+
         if low == 0:
             ret[span(e, cap), :] = eo[span(e, cap), :]
 
@@ -362,8 +407,8 @@
         lanes = lax.broadcasted_iota(jnp.int32, (rows, ep * cap), 1)
         for k, ref in ((0, p0), (1, p1)):
             ref[...] = (lanes == narrow[:, k : k + 1].astype(jnp.int32)).astype(F32).astype(BF16)
-        for load in loads[2:7]:
-            load.wait()
+        loads[2].wait()
+        pltpu.make_async_copy(heads_in, heads_in, w_sem.at[3]).wait()
         here_cos = tab[pl.ds(2 * rows + e, 1), :]
         here_sin = tab[pl.ds(2 * rows + ep + e, 1), :]
         sign = jnp.where(lax.broadcasted_iota(jnp.int32, (BLOCK, hd), 1) < hd // 2, -1.0, 1.0)
@@ -419,15 +464,14 @@
 
     def next_copy():
         return pltpu.make_async_remote_copy(
-            src_ref=state.at[1, :decay_at, :], dst_ref=landed.at[1, :decay_at, :],
+            src_ref=passed.at[0], dst_ref=passed.at[1],
             send_sem=s_send.at[1], recv_sem=s_recv.at[1],
             device_id={"ep": lax.rem(e + 2, ep)}, device_id_type=MESH,
         )
 
     def down_copy():
-        part = landed.at[1, :decay_at, :]
         return pltpu.make_async_remote_copy(
-            src_ref=part, dst_ref=part, send_sem=s_send.at[2], recv_sem=s_recv.at[2],
+            src_ref=passed.at[1], dst_ref=passed.at[1], send_sem=s_send.at[2], recv_sem=s_recv.at[2],
             device_id={"ep": e ^ 1}, device_id_type=MESH,
         )
 
@@ -444,6 +488,7 @@
                 mine = decays(n)[1]
                 state[1, at, :] = mine * landed[0, at, :] + state[0, at, :]
                 excl[0, at, :] = landed[0, at, :]
+            passed[0] = state[1, :decay_at, :].astype(BF16)
 
         if chips > 1:
 
@@ -459,8 +504,8 @@
             for n in range(heads):
                 at = slice(n * hd, (n + 1) * hd)
                 first, mine = decays(n)
-                came = landed[1, at, :]
-                state[1, at, :] = (first * mine) * came + state[1, at, :]
+                came = passed[1, at, :].astype(F32)
+                passed[0, at, :] = ((first * mine) * came + state[1, at, :]).astype(BF16)
                 excl[0, at, :] = first * came + excl[0, at, :]
 
         @pl.when((core == 1) & turn_of & (chip < chips - 1))
@@ -471,7 +516,7 @@
         @pl.when((core == 0) & (chip > 0))
         def _():
             down_copy().wait_recv()
-            excl[0, :decay_at, :] = landed[1, :decay_at, :]
+            excl[0, :decay_at, :] = passed[1].astype(F32)
 
     def retention_close():
         for n in range(heads):
@@ -495,95 +540,128 @@
 
     for load in weight_loads[0]:
         load.wait()
-    z_copy(1, True, True).wait_recv()
-    each(2, g, take_rows)
-    each(2, g, lambda off: row_gather(off).forward())
-    each(2, g, lambda off: row_gather(off).finish())
-    hidden_piece(0, 0)
-    retention_local()
-
-    @pl.when(core == 0)
-    def _():
-        up_copy().start()
-
+
+    def take_partner(u):
+        if units[u][0] <= 1 < units[u][0] + units[u][1]:
+            z_copy(1, True, True).wait_recv()
+        rows_start(u)
+        rows_forward(u)
+        rows_finish(u)
+
+    def hidden(u):
+        for j in range(len(first if u in (0, 2) else cuts)):
+            hidden_piece(u, j)
+
+    def forwards(u):
+        for j in range(len(first if u in (0, 2) else cuts)):
+            forward(u, j)
+
+    take_partner(0)
+    for j in range(len(first) - pieces + 1):
+        hidden_piece(0, j)
     for j in range(1, pieces):
         for load in weight_loads[j]:
             load.wait()
-        hidden_piece(0, j)
+        hidden_piece(0, j + len(first) - pieces)
+    take_partner(1)
+    hidden_piece(1, 0)
+    retention_local()
+
+    @pl.when(core == 0)
+    def _():
+        up_copy().start()
+
+    for j in range(len(first) - 1):
+        forward(0, j)
+    for low, size, whole in units[5:]:
+        group(low, size, 0, d)
+
+
+    @pl.when(jnp.logical_not(opens))
+    def _():
+        z_start(5)
+
+    @pl.when(core == 0)
+    def _():
+        z_start(6)
+
+    forward(0, len(first) - 1)
+    rows_start(2)
+    for j in range(1, pieces):
+        hidden_piece(1, j)
     scan_open()
-    last = full[1][1] - (full[1][1] - full[1][0]) // 2
+
+    @pl.when(opens)
+    def _():
+        z_start(4)
+        z_start(5)
+
+    rows_start(3)
+    rows_forward(2)
+    forward(1, 0)
+    rows_forward(3)
+    rows_finish(2)
+    hidden(2)
+    scan_pass(chip == 1)
 
     @pl.when(core == 1)
     def _():
-        z_start(*full[0], True)
-        z_start(full[1][0], last, True)
-
-    @pl.when(core == 0)
-    def _():
-        z_start(*full[1], True)
-
-
-    each(2 * g, 3 * g, take_rows)
-    each(2 * g, 3 * g, lambda off: row_gather(off).forward())
-    for j in range(pieces):
-        forward(0, j)
-    scan_pass(chip == 1)
-
-    @pl.when(core == 1)
-    def _():
-        z_start(last, full[1][1], True)
-
-    each(2 * g, 3 * g, lambda off: row_gather(off).finish())
-    for j in range(pieces):
-        hidden_piece(1, j)
-
-    each(g, 2 * g, lambda off: z_copy(off, True, True).wait_recv())
-    for j in range(pieces):
-        hidden_piece(2, j)
+        z_start(6)
+
+    for j in range(1, pieces):
+        forward(1, j)
+    rows_finish(3)
+    hidden(3)
     loads[0].wait()
     down(0)
-    forward(1, 0)
+    z_wait(4)
+    hidden(4)
+    forwards(2)
+    down(1)
+    forwards(3)
     scan_pass(chip == 2)
-    for j in range(1, pieces):
-        forward(1, j)
-    forward(2, 0)
-
-    def last_rows(u):
-        low, size = units[u]
-        each(low, low + size, lambda off: z_copy(off, True, True).wait_recv())
-        for j in range(pieces):
-            hidden_piece(u, j)
-
-    last_rows(3)
-    for j in range(1, pieces):
-        forward(2, j)
+    z_start(7)
+    z_wait(5)
+    hidden(5)
+    down(2)
+    forwards(4)
+    down(3)
     scan_pass(chip > 2)
     scan_close()
     retention_close()
     mix_gather(0).start()
-    last_rows(4)
-    down(1)
-    for j in range(pieces):
-        forward(3, j)
-    down(2)
+    z_wait(6)
+    hidden(6)
+    forwards(5)
+    z_wait(7)
+    hidden(7)
+    down(4)
+    forwards(6)
+    down_early(6)
+    down(5)
+    mix_gather(1).start()
+    forwards(7)
     mix_gather(0).forward()
-    for j in range(pieces):
-        forward(4, j)
-    mix_gather(1).start()
-    down(3)
-    down(4)
+    down_early(7)
+    down(6, True)
     mix_gather(1).forward()
+    down(7, True)
     loads[1].wait()
 
-    for b in range(2):
+    def mix_project(b):
         mix_gather(b).finish()
-
-    @pl.loop(0, dq // out_tile)
-    def _(i):
-        cols = pl.ds(pl.multiple_of(i * out_tile, out_tile), out_tile)
-        out_ref[0, :, cols] = dot(ho[...], wo[:, cols]).astype(BF16)
-
-    each(1, ep, lambda off: back_copy(off, True).wait_recv())
+        at = slice(b * half_rows, (b + 1) * half_rows)
+
+        @pl.loop(0, dq // out_tile)
+        def _(i):
+            cols = pl.ds(pl.multiple_of(i * out_tile, out_tile), out_tile)
+            out_ref[0, at, cols] = dot(ho[at, :], wo[:, cols]).astype(BF16)
+
+    def taken(ref, sem):
+        return pltpu.make_async_copy(ref, ref, sem)
+
+    mix_project(0)
+    taken(ret.at[: (ep - 1) * cap, :], r_recv.at[0]).wait()
 
     @pl.loop(0, dq // out_tile)
     def _(i):
@@ -593,22 +671,15 @@
             dot(p0[...], came) * narrow[:, 2:3] + dot(p1[...], came) * narrow[:, 3:4]
         ).astype(BF16)
 
-
-    def drain(low, high, whole):
-        each(low, high, lambda off: z_copy(off, False, whole).wait_send())
-
-    drain(1, 2, True)
-    for low, high in slim:
-        drain(low, high, False)
-        each(low, high, lambda off: row_gather(off).drain())
-    for low, high in full:
-        drain(low, high, True)
-    each(1, ep, lambda off: back_copy(off, False).wait_send())
-    for u in range(len(units)):
-        for j in range(pieces):
-            hid_gather(u, j).drain()
-    for b in range(2):
-        mix_gather(b).drain()
+    mix_project(1)
+
+    slim_rows = sum(offsets(u)[1] - offsets(u)[0] for u in range(4)) * cap
+    taken(og.at[: ep * cap - cap - slim_rows, :], sent.at[0]).wait()
+    taken(og.at[:slim_rows, :dq], sent.at[1]).wait()
+    taken(x.at[:slim_rows, : (tp - 1) * dq], sent.at[2]).wait()
+    taken(h.at[:, : (tp - 1) * fq], sent.at[3]).wait()
+    taken(ho.at[:, : (tp - 1) * heads * hd], sent.at[4]).wait()
+    taken(eo.at[: (ep - 1) * cap, :], sent.at[5]).wait()
 
     @pl.when(core == 0)
     def _():
@@ -645,8 +716,9 @@
     dq = d // tp
     fq = gate_proj.shape[2]
     ff = down_proj.shape[1]
-    slots = max(4, tp - 1)
-    pieces = len(chunk_units(ep)) * 2
+    slots = 2 if tp == 4 else tp - 1
+    units = plan(ep)
+    slim = sum(size for low, size, whole in units if not whole) - 2
     blocks = rows // BLOCK
     srows = heads * hd + 8 * ((heads + 7) // 8)
     vmem = pl.BlockSpec(memory_space=pltpu.VMEM)
@@ -669,10 +741,7 @@
             pltpu.VMEM((d // 128, 128), BF16),
             pltpu.VMEM((2, rows), jnp.int32),
             pltpu.VMEM((2, rows), F32),
-            pltpu.VMEM((rows, width), BF16),
-            pltpu.VMEM((rows, width), BF16),
-            pltpu.VMEM((rows, width), BF16),
-            pltpu.VMEM((rows, width), BF16),
+            pltpu.VMEM((4, rows, width), BF16),
             pltpu.VMEM(table.shape, F32),
             pltpu.VMEM((rows, d), BF16),
             pltpu.VMEM((2, rows, hd), F32),
@@ -690,19 +759,20 @@
             pltpu.VMEM((ep * cap, dq), BF16),
             pltpu.VMEM((rows, width * tp), BF16),
             pltpu.VMEM((2, srows, hd), F32),
-            pltpu.VMEM((2, srows, hd), F32),
+            pltpu.VMEM((1, srows, hd), F32),
+            pltpu.VMEM((2, heads * hd, hd), BF16),
             pltpu.VMEM((blocks, srows, hd), F32),
+            pltpu.VMEM((2, ep // 8 * cap, dq), F32),
             pltpu.VMEM((rows, width), BF16),
             pltpu.VMEM((rows, width), F32),
             pltpu.VMEM((rows, 128), F32),
             pltpu.VMEM((128, rows), F32),
             pltpu.VMEM((rows, 128), F32),
-            dma((17,)),
-            dma((ep,)), dma((ep,)),
-            dma((ep, slots)), dma((ep, slots)),
-            dma((pieces, slots)), dma((pieces, slots)),
-            dma((ep,)), dma((ep,)),
-            dma((2, slots)), dma((2, slots)),
+            dma((14,)), dma((6,)), dma((ep,)),
+            dma((slim, slots)), dma((slim,)),
+            dma((len(units) * 3, slots)), dma((len(units),)),
+            dma((1,)),
+            dma((2, slots)), dma((2,)),
             dma((3,)), dma((3,)),
         ],
         compiler_params=pltpu.CompilerParams(

time: 65 us -> 61.3 us (0.943); the launches traced: 64.8 us -> 60.4 us
  Pallas kernels: 63.3 us -> 58.9 us
    pallas_call x1, Pallas kernels: 63.3 us -> 58.9 us  [on_device(): pl.pallas_call(functools.partial(kernel, ep, tp), out_shape=jax.ShapeDtyp...]
where the time goes in v3:
time: 61.3 us; the launch traced here: 60.4 us
  Pallas kernels  58.9 us (96%)
  local copies, waits for them, and re-layouts  0.82 us (1%)
  between operations  0.64 us (1%)
    pallas_call x1, Pallas kernels, on_device(): pl.pallas_call(functools.partial(kernel, ep, tp), out_shape=jax.ShapeDtyp...  58.9 us

profile of v3, /device:TPU:0, one launch (start us, length us, event | category | flops | bytes accessed | tf_op | source)
XLA Modules:
  0.0 60.4 jit_solution(1472452882949609675)
XLA Ops:
  0.6 58.9 %shard_map.149 = bf16[2,256,512]{2,1,0:T(8,128)(2,1)S(1)} custom-call(bf16[256,512]{1,0:T(8,128)(2,1)} %q_hbm.1, bf16[256,512]{1,0:T(8,128)(2,1)} %k_hbm.1, bf16[256,512]{1,0:T(8,128)(2,1)} %v_hbm.1, bf16[256,512]{1,0:T(8,128)(2,1)} %g_hbm.1, f32[4,256]{1,0:T(4,128)} %bitcast.8, f32[528,128]{1,0:T(8,128)} %constant.2.clone.tab_hbm, ...), custom_call_target="tpu_custom_call" | custom-call | tf_op jit(solution)/shard_map/pallas_call | solution.py:734
  59.6 0.8 %slice_bitcast_fusion = (bf16[256,512]{1,0:T(8,128)(2,1)}, bf16[256,512]{1,0:T(8,128)(2,1)}) fusion(bf16[2,256,512]{2,1,0:T(8,128)(2,1)S(1)} %shard_map.149), kind=kLoop, calls=%fused_computation | loop fusion | bytes 1048576 | tf_op jit(solution)/shard_map/squeeze | solution.py:782

commit v4 on v3

--- a/solution.py
+++ b/solution.py
@@ -88,7 +88,7 @@
     wo_hbm, wg_hbm, wu_hbm, wd_hbm,
     out_ref,
     ld_ref, gain_ref, routes_ref, rw_ref, heads_in, tab, rows_ref, turn,
-    wo, wg, wu, wd, normed, p0, p1, og, x, h, eo, ret, ho, state, landed, passed, excl, partial,
+    wo, wg, wu, wd, normed, p0, p1, late0, late1, og, x, h, eo, ret, ret_late, combined, ho, state, landed, passed, excl, partial, mixed,
     rq, inside, cums, pack, narrow,
     w_sem, sent, z_recv, f_recv, f_hop, h_recv, h_hop, r_recv, m_recv, m_hop, s_send, s_recv,
 ):
@@ -111,6 +111,7 @@
     cuts = [(j * piece, piece) for j in range(pieces)]
     first = [(0, tile), (tile, piece - tile)] * (piece > tile) + cuts[piece > tile :]
     core, chip, chips = lax.rem(e, 2), e // 2, ep // 2
+    inner = lax.rem(chip + chip // 2, 2) == 1
 
     barrier = pltpu.get_barrier_semaphore()
 
@@ -190,8 +191,13 @@
             val = rows_ref[at, cols].astype(F32)
             normed[at, cols] = (val * scale * gain_ref[c : c + 1, :].astype(F32)).astype(BF16)
 
+    late = (6, 7)
+
+    def group_of(low, size):
+        return (e // size) ^ (low // size)
+
     def unit_at(low, size):
-        return span((e // size) ^ (low // size), size * cap)
+        return span(group_of(low, size), size * cap)
 
     def pick(low, size):
         slot = lax.broadcasted_iota(jnp.int32, (size * cap, rows), 0) + (
@@ -243,12 +249,7 @@
         load.start()
     x[span(e, cap), :] = og[span(e, cap), :]
     group(*units[4][:2], 0, d)
-    opens = (core == 1) & (chip == 0)
-
-    @pl.when(jnp.logical_not(opens))
-    def _():
-        z_start(4)
-
+    z_start(4)
 
     slim_at, count = [], 0
     for u in range(4):
@@ -288,8 +289,11 @@
         low, high, _ = offsets(u)
         each(low, high, lambda off: row_gather(u, off).finish())
 
+    counts = [len(first if u in (0, 4) else cuts) for u in range(len(units))]
+    piece_at = [sum(counts[:u]) for u in range(len(units))]
+
     def hid_gather(u, number):
-        start, width = (0, fq) if number is None else (first if u in (0, 2) else cuts)[number]
+        start, width = (0, fq) if number is None else (first if u in (0, 4) else cuts)[number]
         low, size, _ = units[u]
         count = size * cap
         base = ((e // size) ^ (low // size)) * count
@@ -303,14 +307,14 @@
             lambda owner, k: h.at[
                 pl.ds(pl.multiple_of(base + k * (count // 2), count // 2), count // 2), cols(owner)
             ],
-            sent.at[3], lambda slot: h_recv.at[u * 3 + number, slot], h_hop.at[u],
+            sent.at[3], lambda slot: h_recv.at[piece_at[u] + number, slot], h_hop.at[u],
         )
 
     def hid_finish(u):
         if tp == 4:
             hid_gather(u, None).finish()
         else:
-            for j in range(len(first if u in (0, 2) else cuts)):
+            for j in range(len(first if u in (0, 4) else cuts)):
                 hid_gather(u, j).finish()
 
     half_rows = rows // 2
@@ -329,7 +333,7 @@
 
     def hidden_piece(u, j):
         at = unit_at(*units[u][:2])
-        start, width = (first if u in (0, 2) else cuts)[j]
+        start, width = (first if u in (0, 4) else cuts)[j]
 
         @pl.loop(0, width // tile)
         def _(i):
@@ -342,15 +346,49 @@
 
         hid_gather(u, j).start()
 
-    def back_copy(off, cols):
+    def back_copy(u, off, cols):
         other = e ^ off
+        size = units[u][1]
+        if u in late:
+            row = late.index(u) * size + lax.rem(e, size)
+            dst = ret_late.at[pl.ds(pl.multiple_of(row * cap, cap), cap), cols]
+        else:
+            dst = ret.at[span(e, cap), cols]
         return pltpu.make_async_remote_copy(
-            src_ref=eo.at[span(other, cap), cols], dst_ref=ret.at[span(e, cap), cols],
-            send_sem=sent.at[5], recv_sem=r_recv.at[0],
+            src_ref=eo.at[span(other, cap), cols], dst_ref=dst,
+            send_sem=sent.at[5], recv_sem=r_recv.at[1 if u in late else 0],
             device_id={"ep": other}, device_id_type=MESH,
         )
 
     out_tile = min(256, dq)
+
+    def mix_early(b):
+        if tp == 4:
+            at = slice(b * half_rows, (b + 1) * half_rows)
+            share = heads * hd
+
+            @pl.loop(0, dq // out_tile)
+            def _(i):
+                cols = pl.ds(pl.multiple_of(i * out_tile, out_tile), out_tile)
+                mixed[at, cols] = sum(
+                    dot(ho[at, span(t ^ k, share)], wo[span(t ^ k, share), cols]) for k in range(3)
+                )
+
+    def mix_project(b):
+        mix_gather(b).finish()
+        at = slice(b * half_rows, (b + 1) * half_rows)
+        share = heads * hd
+
+        @pl.loop(0, dq // out_tile)
+        def _(i):
+            cols = pl.ds(pl.multiple_of(i * out_tile, out_tile), out_tile)
+            if tp == 4:
+                total = mixed[at, cols] + dot(
+                    ho[at, span(t ^ 3, share)], wo[span(t ^ 3, share), cols]
+                )
+            else:
+                total = dot(ho[at, :], wo[:, cols])
+            out_ref[0, at, cols] = total.astype(BF16)
 
     def down_early(u):
         if tp == 4:
@@ -379,7 +417,7 @@
             else:
                 total = dot(h[at, :], wd[:, cols])
             eo[at, cols] = total.astype(BF16)
-            each(max(1, low), low + size, lambda off: back_copy(off, cols).start())
+            each(max(1, low), low + size, lambda off: back_copy(u, off, cols).start())
 
         if low == 0:
             ret[span(e, cap), :] = eo[span(e, cap), :]
@@ -407,6 +445,14 @@
         lanes = lax.broadcasted_iota(jnp.int32, (rows, ep * cap), 1)
         for k, ref in ((0, p0), (1, p1)):
             ref[...] = (lanes == narrow[:, k : k + 1].astype(jnp.int32)).astype(F32).astype(BF16)
+        count = units[late[0]][1] * cap
+        place = lax.broadcasted_iota(jnp.int32, (rows, 2 * count), 1)
+        bases = [group_of(*units[u][:2]) * count for u in late]
+        slot = jnp.where(place < count, place + bases[0], place - count + bases[1])
+        for k, ref in ((0, late0), (1, late1)):
+            ref[...] = (slot == narrow[:, k : k + 1].astype(jnp.int32)).astype(F32).astype(BF16)
+        for u in late:
+            ret[unit_at(*units[u][:2]), :] = jnp.zeros((count, dq), BF16)
         loads[2].wait()
         pltpu.make_async_copy(heads_in, heads_in, w_sem.at[3]).wait()
         here_cos = tab[pl.ds(2 * rows + e, 1), :]
@@ -549,11 +595,11 @@
         rows_finish(u)
 
     def hidden(u):
-        for j in range(len(first if u in (0, 2) else cuts)):
+        for j in range(len(first if u in (0, 4) else cuts)):
             hidden_piece(u, j)
 
     def forwards(u):
-        for j in range(len(first if u in (0, 2) else cuts)):
+        for j in range(len(first if u in (0, 4) else cuts)):
             forward(u, j)
 
     take_partner(0)
@@ -577,13 +623,11 @@
         group(low, size, 0, d)
 
 
-    @pl.when(jnp.logical_not(opens))
+    early = jnp.logical_not(inner) & (core == 0)
+
+    @pl.when(early)
     def _():
         z_start(5)
-
-    @pl.when(core == 0)
-    def _():
-        z_start(6)
 
     forward(0, len(first) - 1)
     rows_start(2)
@@ -591,51 +635,65 @@
         hidden_piece(1, j)
     scan_open()
 
-    @pl.when(opens)
-    def _():
-        z_start(4)
+    rows_start(3)
+
+    @pl.when(jnp.logical_not(early))
+    def _():
         z_start(5)
 
-    rows_start(3)
+    @pl.when(core == 0)
+    def _():
+        z_start(6)
+
+    forward(1, 0)
     rows_forward(2)
-    forward(1, 0)
+    for j in range(1, pieces):
+        forward(1, j)
+    z_wait(4)
+    hidden(4)
+    scan_pass(chip == 1)
+
+    @pl.when(core == 1)
+    def _():
+        z_start(6)
+
     rows_forward(3)
     rows_finish(2)
     hidden(2)
-    scan_pass(chip == 1)
-
-    @pl.when(core == 1)
-    def _():
-        z_start(6)
-
-    for j in range(1, pieces):
-        forward(1, j)
+    forwards(4)
     rows_finish(3)
     hidden(3)
+
+    @pl.when(core == 0)
+    def _():
+        z_start(7)
+
     loads[0].wait()
     down(0)
-    z_wait(4)
-    hidden(4)
     forwards(2)
+    z_wait(5)
+    for j in range(pieces):
+        hidden_piece(5, j)
+        forward(3, j)
+    scan_pass(chip == 2)
+
+    @pl.when(core == 1)
+    def _():
+        z_start(7)
+
     down(1)
-    forwards(3)
-    scan_pass(chip == 2)
-    z_start(7)
-    z_wait(5)
-    hidden(5)
-    down(2)
-    forwards(4)
-    down(3)
     scan_pass(chip > 2)
     scan_close()
     retention_close()
     mix_gather(0).start()
+    down(4)
     z_wait(6)
     hidden(6)
     forwards(5)
+    down(2)
     z_wait(7)
     hidden(7)
-    down(4)
+    down(3)
     forwards(6)
     down_early(6)
     down(5)
@@ -644,34 +702,38 @@
     mix_gather(0).forward()
     down_early(7)
     down(6, True)
+    loads[1].wait()
+    mix_early(0)
     mix_gather(1).forward()
-    down(7, True)
-    loads[1].wait()
-
-    def mix_project(b):
-        mix_gather(b).finish()
-        at = slice(b * half_rows, (b + 1) * half_rows)
-
-        @pl.loop(0, dq // out_tile)
-        def _(i):
-            cols = pl.ds(pl.multiple_of(i * out_tile, out_tile), out_tile)
-            out_ref[0, at, cols] = dot(ho[at, :], wo[:, cols]).astype(BF16)
+    mix_early(1)
 
     def taken(ref, sem):
         return pltpu.make_async_copy(ref, ref, sem)
 
-    mix_project(0)
-    taken(ret.at[: (ep - 1) * cap, :], r_recv.at[0]).wait()
+    def weighed(first_pick, second_pick, came):
+        return (
+            dot(first_pick[...], came) * narrow[:, 2:3]
+            + dot(second_pick[...], came) * narrow[:, 3:4]
+        )
+
+    taken(ret.at[: (ep - 1) * cap - ret_late.shape[0], :], r_recv.at[0]).wait()
 
     @pl.loop(0, dq // out_tile)
     def _(i):
         cols = pl.ds(pl.multiple_of(i * out_tile, out_tile), out_tile)
-        came = ret[:, cols]
+        combined[:, cols] = weighed(p0, p1, ret[:, cols])
+
+    down(7, True)
+    mix_project(0)
+    mix_project(1)
+    taken(ret_late, r_recv.at[1]).wait()
+
+    @pl.loop(0, dq // out_tile)
+    def _(i):
+        cols = pl.ds(pl.multiple_of(i * out_tile, out_tile), out_tile)
         out_ref[1, :, cols] = (
-            dot(p0[...], came) * narrow[:, 2:3] + dot(p1[...], came) * narrow[:, 3:4]
+            combined[:, cols] + weighed(late0, late1, ret_late[:, cols])
         ).astype(BF16)
-
-    mix_project(1)
 
     slim_rows = sum(offsets(u)[1] - offsets(u)[0] for u in range(4)) * cap
     taken(og.at[: ep * cap - cap - slim_rows, :], sent.at[0]).wait()
@@ -752,17 +814,22 @@
             pltpu.VMEM((rows, d), BF16),
             pltpu.VMEM((rows, ep * cap), BF16),
             pltpu.VMEM((rows, ep * cap), BF16),
+            pltpu.VMEM((rows, ep // 4 * cap), BF16),
+            pltpu.VMEM((rows, ep // 4 * cap), BF16),
             pltpu.VMEM((ep * cap, d), BF16),
             pltpu.VMEM((ep * cap, d), BF16),
             pltpu.VMEM((ep * cap, ff), BF16),
             pltpu.VMEM((ep * cap, dq), BF16),
             pltpu.VMEM((ep * cap, dq), BF16),
+            pltpu.VMEM((ep // 4 * cap, dq), BF16),
+            pltpu.VMEM((rows, dq), F32),
             pltpu.VMEM((rows, width * tp), BF16),
             pltpu.VMEM((2, srows, hd), F32),
             pltpu.VMEM((1, srows, hd), F32),
             pltpu.VMEM((2, heads * hd, hd), BF16),
             pltpu.VMEM((blocks, srows, hd), F32),
             pltpu.VMEM((2, ep // 8 * cap, dq), F32),
+            pltpu.VMEM((rows, dq), F32),
             pltpu.VMEM((rows, width), BF16),
             pltpu.VMEM((rows, width), F32),
             pltpu.VMEM((rows, 128), F32),
@@ -770,8 +837,8 @@
             pltpu.VMEM((rows, 128), F32),
             dma((14,)), dma((6,)), dma((ep,)),
             dma((slim, slots)), dma((slim,)),
-            dma((len(units) * 3, slots)), dma((len(units),)),
-            dma((1,)),
+            dma((len(units) * 2 + 2, slots)), dma((len(units),)),
+            dma((2,)),
             dma((2, slots)), dma((2,)),
             dma((3,)), dma((3,)),
         ],

time: 61.3 us -> 60 us (0.979)
  Pallas kernels: 58.9 us -> 58 us
    pallas_call x1, Pallas kernels: 58.9 us -> 58 us  [on_device(): pl.pallas_call(functools.partial(kernel, ep, tp), out_shape=jax.ShapeDtyp...]
where the time goes in v4:
time: 60 us; the launch traced here: 59.5 us
  Pallas kernels  58 us (97%)
  local copies, waits for them, and re-layouts  0.82 us (1%)
  between operations  0.64 us (1%)
    pallas_call x1, Pallas kernels, on_device(): pl.pallas_call(functools.partial(kernel, ep, tp), out_shape=jax.ShapeDtyp...  58 us

profile of v4, /device:TPU:0, one launch (start us, length us, event | category | flops | bytes accessed | tf_op | source)
XLA Modules:
  0.0 59.5 jit_solution(10285258571622423307)
XLA Ops:
  0.6 58.0 %shard_map.149 = bf16[2,256,512]{2,1,0:T(8,128)(2,1)S(1)} custom-call(bf16[256,512]{1,0:T(8,128)(2,1)} %q_hbm.1, bf16[256,512]{1,0:T(8,128)(2,1)} %k_hbm.1, bf16[256,512]{1,0:T(8,128)(2,1)} %v_hbm.1, bf16[256,512]{1,0:T(8,128)(2,1)} %g_hbm.1, f32[4,256]{1,0:T(4,128)} %bitcast.8, f32[528,128]{1,0:T(8,128)} %constant.2.clone.tab_hbm, ...), custom_call_target="tpu_custom_call" | custom-call | tf_op jit(solution)/shard_map/pallas_call | solution.py:796
  58.7 0.8 %slice_bitcast_fusion = (bf16[256,512]{1,0:T(8,128)(2,1)}, bf16[256,512]{1,0:T(8,128)(2,1)}) fusion(bf16[2,256,512]{2,1,0:T(8,128)(2,1)S(1)} %shard_map.149), kind=kLoop, calls=%fused_computation | loop fusion | bytes 1048576 | tf_op jit(solution)/shard_map/squeeze | solution.py:849

commit v5 on v4

--- a/solution.py
+++ b/solution.py
@@ -671,6 +671,16 @@
     loads[0].wait()
     down(0)
     forwards(2)
+
+    def close():
+        scan_close()
+        retention_close()
+        mix_gather(0).start()
+
+    @pl.when(chip < 2)
+    def _():
+        close()
+
     z_wait(5)
     for j in range(pieces):
         hidden_piece(5, j)
@@ -682,13 +692,26 @@
         z_start(7)
 
     down(1)
+    ends = chip == chips - 1
+
+    @pl.when(ends)
+    def _():
+        z_wait(6)
+        hidden(6)
+
     scan_pass(chip > 2)
-    scan_close()
-    retention_close()
-    mix_gather(0).start()
+
+    @pl.when(chip >= 2)
+    def _():
+        close()
+
     down(4)
-    z_wait(6)
-    hidden(6)
+
+    @pl.when(jnp.logical_not(ends))
+    def _():
+        z_wait(6)
+        hidden(6)
+
     forwards(5)
     down(2)
     z_wait(7)

time: 60 us -> 58.7 us (0.978)
  Pallas kernels: 58 us -> 57.1 us
    pallas_call x1, Pallas kernels: 58 us -> 57.1 us  [on_device(): pl.pallas_call(functools.partial(kernel, ep, tp), out_shape=jax.ShapeDtyp...]
where the time goes in v5:
time: 58.7 us; the launch traced here: 58.6 us
  Pallas kernels  57.1 us (97%)
  local copies, waits for them, and re-layouts  0.82 us (1%)
  between operations  0.64 us (1%)
    pallas_call x1, Pallas kernels, on_device(): pl.pallas_call(functools.partial(kernel, ep, tp), out_shape=jax.ShapeDtyp...  57.1 us

profile of v5, /device:TPU:0, one launch (start us, length us, event | category | flops | bytes accessed | tf_op | source)
XLA Modules:
  0.0 58.6 jit_solution(2612794853842717289)
XLA Ops:
  0.6 57.1 %shard_map.149 = bf16[2,256,512]{2,1,0:T(8,128)(2,1)S(1)} custom-call(bf16[256,512]{1,0:T(8,128)(2,1)} %q_hbm.1, bf16[256,512]{1,0:T(8,128)(2,1)} %k_hbm.1, bf16[256,512]{1,0:T(8,128)(2,1)} %v_hbm.1, bf16[256,512]{1,0:T(8,128)(2,1)} %g_hbm.1, f32[4,256]{1,0:T(4,128)} %bitcast.8, f32[528,128]{1,0:T(8,128)} %constant.2.clone.tab_hbm, ...), custom_call_target="tpu_custom_call" | custom-call | tf_op jit(solution)/shard_map/pallas_call | solution.py:819
  57.8 0.8 %slice_bitcast_fusion = (bf16[256,512]{1,0:T(8,128)(2,1)}, bf16[256,512]{1,0:T(8,128)(2,1)}) fusion(bf16[2,256,512]{2,1,0:T(8,128)(2,1)S(1)} %shard_map.149), kind=kLoop, calls=%fused_computation | loop fusion | bytes 1048576 | tf_op jit(solution)/shard_map/squeeze | solution.py:872

commit v6 on v5

--- a/solution.py
+++ b/solution.py
@@ -289,11 +289,11 @@
         low, high, _ = offsets(u)
         each(low, high, lambda off: row_gather(u, off).finish())
 
-    counts = [len(first if u in (0, 4) else cuts) for u in range(len(units))]
+    counts = [len(first if u in (0, 4, 5) else cuts) for u in range(len(units))]
     piece_at = [sum(counts[:u]) for u in range(len(units))]
 
     def hid_gather(u, number):
-        start, width = (0, fq) if number is None else (first if u in (0, 4) else cuts)[number]
+        start, width = (0, fq) if number is None else (first if u in (0, 4, 5) else cuts)[number]
         low, size, _ = units[u]
         count = size * cap
         base = ((e // size) ^ (low // size)) * count
@@ -314,7 +314,7 @@
         if tp == 4:
             hid_gather(u, None).finish()
         else:
-            for j in range(len(first if u in (0, 4) else cuts)):
+            for j in range(len(first if u in (0, 4, 5) else cuts)):
                 hid_gather(u, j).finish()
 
     half_rows = rows // 2
@@ -333,7 +333,7 @@
 
     def hidden_piece(u, j):
         at = unit_at(*units[u][:2])
-        start, width = (first if u in (0, 4) else cuts)[j]
+        start, width = (first if u in (0, 4, 5) else cuts)[j]
 
         @pl.loop(0, width // tile)
         def _(i):
@@ -595,11 +595,11 @@
         rows_finish(u)
 
     def hidden(u):
-        for j in range(len(first if u in (0, 4) else cuts)):
+        for j in range(len(first if u in (0, 4, 5) else cuts)):
             hidden_piece(u, j)
 
     def forwards(u):
-        for j in range(len(first if u in (0, 4) else cuts)):
+        for j in range(len(first if u in (0, 4, 5) else cuts)):
             forward(u, j)
 
     take_partner(0)
@@ -682,8 +682,11 @@
         close()
 
     z_wait(5)
+    more = len(first) - pieces
+    for j in range(more):
+        hidden_piece(5, j)
     for j in range(pieces):
-        hidden_piece(5, j)
+        hidden_piece(5, j + more)
         forward(3, j)
     scan_pass(chip == 2)
 
@@ -860,7 +863,7 @@
             pltpu.VMEM((rows, 128), F32),
             dma((14,)), dma((6,)), dma((ep,)),
             dma((slim, slots)), dma((slim,)),
-            dma((len(units) * 2 + 2, slots)), dma((len(units),)),
+            dma((len(units) * 2 + 3, slots)), dma((len(units),)),
             dma((2,)),
             dma((2, slots)), dma((2,)),
             dma((3,)), dma((3,)),

time: 58.7 us -> 58.7 us (level)
  no operation moved by 1% of the time
where the time goes in v6:
time: 58.7 us; the launch traced here: 58.6 us
  Pallas kernels  57.1 us (97%)
  local copies, waits for them, and re-layouts  0.82 us (1%)
  between operations  0.64 us (1%)
    pallas_call x1, Pallas kernels, on_device(): pl.pallas_call(functools.partial(kernel, ep, tp), out_shape=jax.ShapeDtyp...  57.1 us

profile of v6, /device:TPU:0, one launch (start us, length us, event | category | flops | bytes accessed | tf_op | source)
XLA Modules:
  0.0 58.6 jit_solution(256764547545863981)
XLA Ops:
  0.6 57.1 %shard_map.149 = bf16[2,256,512]{2,1,0:T(8,128)(2,1)S(1)} custom-call(bf16[256,512]{1,0:T(8,128)(2,1)} %q_hbm.1, bf16[256,512]{1,0:T(8,128)(2,1)} %k_hbm.1, bf16[256,512]{1,0:T(8,128)(2,1)} %v_hbm.1, bf16[256,512]{1,0:T(8,128)(2,1)} %g_hbm.1, f32[4,256]{1,0:T(4,128)} %bitcast.8, f32[528,128]{1,0:T(8,128)} %constant.2.clone.tab_hbm, ...), custom_call_target="tpu_custom_call" | custom-call | tf_op jit(solution)/shard_map/pallas_call | solution.py:822
  57.8 0.8 %slice_bitcast_fusion = (bf16[256,512]{1,0:T(8,128)(2,1)}, bf16[256,512]{1,0:T(8,128)(2,1)}) fusion(bf16[2,256,512]{2,1,0:T(8,128)(2,1)S(1)} %shard_map.149), kind=kLoop, calls=%fused_computation | loop fusion | bytes 1048576 | tf_op jit(solution)/shard_map/squeeze | solution.py:875
